TPU v7x, 512 devices: a whole 4x8x8 slice. The times are simulated.
512 devices in a mesh: rep: 2 (over z_hi), fs: 32 (over z_lo, y), tp: 8 (over x, core).
Axes of the slice: x: 4, y: 8, z: 8 (z_hi: 2, z_lo: 4; z = z_hi * 4 + z_lo), core: 2. Of those that a mesh axis runs over, the one named last changes fastest.
Arguments:
- late_rows: bfloat16 [16384, 2048], P(('rep', 'fs')), parts along dimension 0, may hold values from -6 to 6
- early_rows: bfloat16 [16384, 2048], P(('rep', 'fs')), parts along dimension 0, may hold values from -6 to 6
- hidden_cot: bfloat16 [16384, 5632], P(('rep', 'fs'), 'tp'), parts along dimension 0, may hold values from -6 to 6
- gate_weight: bfloat16 [2048, 5632], P('fs', 'tp'), may hold values from -0.125 to 0.125
- up_weight: bfloat16 [2048, 5632], P('fs', 'tp'), may hold values from -0.125 to 0.125
- gate_taps: bfloat16 [3, 5632], P(None, 'tp'), may hold values from -3.5 to 3.5
- up_taps: bfloat16 [3, 5632], P(None, 'tp'), may hold values from -3.5 to 3.5
- gate_grad_sum: float32 [4096, 5632], P(('rep', 'fs'), 'tp'), parts along dimension 0, may hold values from -6 to 6
- up_grad_sum: float32 [4096, 5632], P(('rep', 'fs'), 'tp'), parts along dimension 0, may hold values from -6 to 6
- gate_taps_sum: float32 [6, 5632], P('rep', 'tp'), parts along dimension 0, may hold values from -6 to 6
- up_taps_sum: float32 [6, 5632], P('rep', 'tp'), parts along dimension 0, may hold values from -6 to 6
Outputs:
- late_hidden: bfloat16 [16384, 5632], P(('rep', 'fs'), 'tp'), parts along dimension 0
- early_grad: bfloat16 [16384, 2048], P(('rep', 'fs')), parts along dimension 0
- gate_grad_next: float32 [4096, 5632], P(('rep', 'fs'), 'tp'), parts along dimension 0
- up_grad_next: float32 [4096, 5632], P(('rep', 'fs'), 'tp'), parts along dimension 0
- gate_taps_next: float32 [6, 5632], P('rep', 'tp'), parts along dimension 0
- up_taps_next: float32 [6, 5632], P('rep', 'tp'), parts along dimension 0
There are 2 independent parts, one for each index of `rep`. A program takes and returns all parts, laid end to end along the dimension named above; an argument that names none is the same for every part. Nothing has to cross between parts.
All inputs are finite; a program needn't handle non-finite values.
Results may differ from a plain program's by a relative error of at most 0.02.
Values may be sent and summed in bfloat16 or wider, within the bound.
A program may use at most 64 MiB of HBM per device.

v0:
```python
import jax
import jax.numpy as jnp
from jax import lax
from jax.sharding import Mesh
from jax.sharding import PartitionSpec as P

FS = ("fs_0", "fs_1")
REP_FS = ("rep", "fs_0", "fs_1")


contract_last = (((1,), (1,)), ((), ()))
contract_first = (((0,), (0,)), ((), ()))


def in_order(pieces, dim):
    pieces = jnp.moveaxis(pieces, 0, dim)
    dims = pieces.shape
    return pieces.reshape(*dims[:dim], dims[dim] * dims[dim + 1], *dims[dim + 2 :])


def all_blocks(array, axes, order):
    pieces = array
    for k in order:
        pieces = lax.all_gather(pieces, axes[k])
    done = order[::-1]
    back = [done.index(k) for k in range(len(axes))]
    pieces = pieces.transpose(*back, *range(len(axes), pieces.ndim))
    return pieces.reshape(-1, *array.shape)


def whole_of(array, axes, order, dim):
    return in_order(all_blocks(array, axes, order), dim)


def cut_along(array, dim, size):
    before, after = (array.shape[:dim], array.shape[dim + 1 :])
    return jnp.moveaxis(array.reshape(*before, size, -1, *after), dim, 0)


def sent_and_summed(array, axis, dim):
    size = lax.axis_size(axis)
    pieces = lax.all_to_all(cut_along(array, dim, size), axis, 0, 0, tiled=True)
    return jnp.sum(pieces.astype(jnp.float32), axis=0)


def copy_for_each(array, axis):
    size = lax.axis_size(axis)
    return lax.all_to_all(
        jnp.broadcast_to(array[None], (size, *array.shape)), axis, 0, 0, tiled=True
    )


def gathered_copies(array, axis, dim):
    pieces = copy_for_each(array, axis)
    return in_order(pieces, dim)


def reduced_to_own(pieces, axes, order):
    inside = pieces.shape[1:]
    pieces = pieces.reshape(*(lax.axis_size(a) for a in axes), *inside)
    pieces = jnp.moveaxis(pieces, order, range(len(axes))).reshape(-1, *inside)
    for k in order:
        pieces = lax.psum_scatter(pieces, axes[k], scatter_dimension=0, tiled=True)
    return pieces[0]


def summed_rows(array, axes, order, dim):
    size = lax.axis_size(axes)
    return reduced_to_own(cut_along(array, dim, size), axes, order)


def taken_together(array, axis):
    everything = copy_for_each(array, axis)
    return jnp.sum(everything, axis=0)


def in_one(arrays, axis):
    ends = [0]
    for a in arrays:
        ends.append(ends[-1] + a.size)
    subtotal = taken_together(jnp.concatenate([a.ravel() for a in arrays]), axis)
    return tuple((subtotal[b:e].reshape(a.shape) for a, b, e in zip(arrays, ends, ends[1:])))


def causal_mix(values, filter_taps):
    length = values.shape[-2]
    widths = [(0, 0)] * values.ndim
    widths[-2] = (2, 0)
    padded = jnp.pad(values, widths)
    return (
        filter_taps[0] * padded[..., 0:length, :]
        + filter_taps[1] * padded[..., 1 : length + 1, :]
        + filter_taps[2] * padded[..., 2 : length + 2, :]
    )


def mix_back(grads, filter_taps):
    length = grads.shape[-2]
    widths = [(0, 0)] * grads.ndim
    widths[-2] = (0, 2)
    padded = jnp.pad(grads, widths)
    return (
        filter_taps[2] * padded[..., 0:length, :]
        + filter_taps[1] * padded[..., 1 : length + 1, :]
        + filter_taps[0] * padded[..., 2 : length + 2, :]
    )


def tap_products(grads, values):
    length = values.shape[-2]
    widths = [(0, 0)] * values.ndim
    widths[-2] = (2, 0)
    padded = jnp.pad(values, widths)
    axes = tuple(range(values.ndim - 1))
    return jnp.stack(
        [
            jnp.sum(grads * padded[..., offset : offset + length, :], axis=axes)
            for offset in range(3)
        ]
    )


def stored(product):
    return lax.optimization_barrier(product.astype(jnp.bfloat16)).astype(jnp.float32)


def per_device(
    late_rows,
    early_rows,
    hidden_cot,
    gate_weight,
    up_weight,
    gate_taps,
    up_taps,
    gate_grad_sum,
    up_grad_sum,
    gate_taps_sum,
    up_taps_sum,
):
    row_count = late_rows.shape[0]
    width_local = gate_weight.shape[1]
    rows_scale = (row_count * lax.axis_size(FS)) ** (-0.5)
    gate_filter = gate_taps.astype(jnp.float32)
    up_filter = up_taps.astype(jnp.float32)
    joined_weight = jnp.concatenate([gate_weight, up_weight], axis=1)
    both_rows = jnp.concatenate([late_rows, early_rows], axis=0)
    whole_joined = whole_of(joined_weight, FS, (0, 1), 0)
    projected = jnp.dot(both_rows, whole_joined, preferred_element_type=jnp.float32)
    projected = stored(projected)
    late_gate = projected[:row_count, :width_local]
    late_up = projected[:row_count, width_local:]
    early_gate = projected[row_count:, :width_local]
    early_up = projected[row_count:, width_local:]
    late_hidden = (
        jax.nn.gelu(causal_mix(late_gate, gate_filter), approximate=True)
        * causal_mix(late_up, up_filter)
    ).astype(jnp.bfloat16)
    gate_mix = causal_mix(early_gate, gate_filter)
    up_mix = causal_mix(early_up, up_filter)
    cotangent = hidden_cot.astype(jnp.float32)
    activated, gelu_back = jax.vjp(
        lambda mixed_value: jax.nn.gelu(mixed_value, approximate=True), gate_mix
    )
    d_gate_mix = gelu_back(cotangent * up_mix)[0]
    d_up_mix = cotangent * activated
    d_gate_pre = mix_back(d_gate_mix, gate_filter).astype(jnp.bfloat16)
    d_up_pre = mix_back(d_up_mix, up_filter).astype(jnp.bfloat16)
    both_grads = jnp.concatenate([d_gate_pre, d_up_pre], axis=1)
    own_rows = sent_and_summed(
        lax.dot_general(
            both_grads, whole_joined, contract_last, preferred_element_type=jnp.float32
        ).astype(jnp.bfloat16),
        "tp",
        0,
    )
    early_grad = gathered_copies(own_rows.astype(jnp.bfloat16), "tp", 0)
    summed = summed_rows(
        (
            lax.dot_general(
                early_rows, both_grads, contract_first, preferred_element_type=jnp.float32
            )
            * rows_scale
        ).astype(jnp.bfloat16),
        FS,
        (1, 0),
        0,
    ).astype(jnp.float32)
    gate_tap_sums, up_tap_sums = in_one(
        (
            rows_scale * tap_products(d_gate_mix, early_gate),
            rows_scale * tap_products(d_up_mix, early_up),
        ),
        FS,
    )
    return (
        late_hidden,
        early_grad,
        gate_grad_sum + summed[:, :width_local],
        up_grad_sum + summed[:, width_local:],
        gate_taps_sum + gate_tap_sums,
        up_taps_sum + up_tap_sums,
    )


def solution(mesh):
    split = Mesh(
        mesh.devices.reshape(mesh.shape["rep"], 4, 8, mesh.shape["tp"]),
        ("rep", "fs_0", "fs_1", "tp"),
    )
    placed = (
        P(REP_FS, None),
        P(REP_FS, None),
        P(REP_FS, "tp"),
        P(FS, "tp"),
        P(FS, "tp"),
        P(None, "tp"),
        P(None, "tp"),
        P(REP_FS, "tp"),
        P(REP_FS, "tp"),
        P("rep", "tp"),
        P("rep", "tp"),
    )
    return jax.shard_map(
        per_device,
        mesh=split,
        in_specs=placed,
        out_specs=(
            P(REP_FS, "tp"),
            P(REP_FS, None),
            P(REP_FS, "tp"),
            P(REP_FS, "tp"),
            P("rep", "tp"),
            P("rep", "tp"),
        ),
        check_vma=False,
    )
```

profile of v0, /device:TPU:6, one launch (start us, length us, event | category | flops | bytes accessed | tf_op | source)
XLA Modules:
  0.0 258.7 jit_solution(8951374495315372138)
XLA Ops:
  7.2 0.0 all-gather.4.cloned.1.call-start
  7.2 1.0 pad_maximum_fusion.3
  8.3 21.9 %all-gather = bf16[256,1408]{1,0:T(8,128)(2,1)} all-gather(bf16[64,1408]{1,0:T(8,128)(2,1)S(1)} %pad_maximum_fusion.3), channel_id=2, replica_groups=mesh['rep'=2,'fs_0'=4,'fs_1'=8,'tp'=8] {'fs_0'}, dimensions={0}, use_global_device_ids=true | all-gather | bytes 901120 | tf_op jit(solution)/shard_map/all_gather | solution.py:24
  30.1 0.0 all-gather.4.cloned.1.call-update
  30.2 0.0 reduce-scatter.3.cloned.1.call-start
  30.2 0.7 convert_element_type.51
  30.9 0.7 convert_element_type.54
  31.6 1.2 copy.39
  32.8 0.1 slice_reduce_fusion.2
  32.8 71.0 %all-gather.4.cloned.1.call-done = bf16[32,64,1408]{2,1,0:T(8,128)(2,1)} async-done(((bf16[4,64,1408]{2,1,0:T(8,128)(2,1)}), bf16[32,64,1408]{2,1,0:T(8,128)(2,1)}) %all-gather.4.cloned.1.call-update) | async-done | bytes 5767184 | tf_op jit(solution)/shard_map/all_gather | solution.py:24
  103.8 3.3 %copy.38 = bf16[4,8,64,1408]{3,2,1,0:T(8,128)(2,1)S(1)} copy(bf16[4,8,64,1408]{3,2,0,1:T(8,128)(2,1)} %bitcast.23) | data formatting | bytes 11534336 | tf_op jit(solution)/shard_map/transpose | solution.py:27
  107.1 3.4 %convolution_convert_fusion = bf16[512,1408]{1,0:T(8,128)(2,1)S(1)} fusion(bf16[2048,1408]{1,0:T(8,128)(2,1)S(1)} %bitcast.21, bf16[256,2048]{1,0:T(8,128)(2,1)S(1)} %copy-done.6, bf16[256,2048]{1,0:T(8,128)(2,1)S(1)} %copy-done.5), kind=kOutput, calls=%fused_computation.2 | convolution fusion | flops 2957705216 | bytes 9306112 | tf_op jit(solution)/shard_map/dot_general | solution.py:148
  110.6 0.2 convert_element_type.53
  110.8 0.4 fusion.23
  111.2 1.8 multiply_reduce_fusion.5
  113.1 1.2 add_convert_fusion.1
  114.3 4.4 %fusion = bf16[2048,1408]{0,1:T(8,128)(2,1)} fusion(bf16[256,2048]{1,0:T(8,128)(2,1)S(1)} %copy-done.6, bf16[256,704]{1,0:T(8,128)(2,1)S(1)} %get-tuple-element.72, bf16[256,704]{1,0:T(8,128)(2,1)S(1)} %get-tuple-element.70), kind=kOutput, calls=%fused_computation.1 | convolution fusion | flops 1483603968 | bytes 7536640 | tf_op jit(solution)/shard_map/dot_general | solution.py:179
  118.7 8.4 %copy.40 = bf16[2048,1408]{1,0:T(8,128)(2,1)} copy(bf16[2048,1408]{0,1:T(8,128)(2,1)} %fusion) | data formatting | bytes 11534336 | tf_op jit(solution)/shard_map/convert_element_type | solution.py:183
  127.1 5.8 %copy.41 = bf16[8,4,64,1408]{3,2,1,0:T(8,128)(2,1)} copy(bf16[8,4,64,1408]{3,2,0,1:T(8,128)(2,1)} %bitcast.20) | data formatting | bytes 11534336 | tf_op jit(solution)/shard_map/transpose | solution.py:61
  132.8 0.0 reduce-scatter.3.cloned.1.call-update
  132.8 5.4 %convolution_convert_fusion.1 = bf16[256,2048]{1,0:T(8,128)(2,1)} fusion(bf16[2048,1408]{1,0:T(8,128)(2,1)} %bitcast.22, bf16[256,704]{1,0:T(8,128)(2,1)S(1)} %get-tuple-element.72, bf16[256,704]{1,0:T(8,128)(2,1)S(1)} %get-tuple-element.70), kind=kOutput, calls=%fused_computation.3 | convolution fusion | flops 1478361088 | bytes 7536640 | tf_op jit(solution)/shard_map/dot_general | solution.py:170
  138.3 4.8 %all-to-all-start = ((bf16[8,32,2048]{2,1,0:T(8,128)(2,1)}), bf16[8,32,2048]{2,1,0:T(8,128)(2,1)S(1)}, u32[]{:S(2)}, u32[]{:S(2)}) async-start(bf16[8,32,2048]{2,1,0:T(8,128)(2,1)} %bitcast.4), calls=%async_computation | async-start | bytes 2097152 | tf_op jit(solution)/shard_map/all_to_all | solution.py:42
  143.1 0.0 copy-start.3
  143.1 0.1 mul.299
  143.2 0.1 mul.294
  143.3 0.1 pad_maximum_fusion.4
  143.4 13.5 %all-to-all-done = bf16[8,32,2048]{2,1,0:T(8,128)(2,1)S(1)} async-done(((bf16[8,32,2048]{2,1,0:T(8,128)(2,1)}), bf16[8,32,2048]{2,1,0:T(8,128)(2,1)S(1)}, u32[]{:S(2)}, u32[]{:S(2)}) %all-to-all-start) | async-done | bytes 1048608 | tf_op jit(solution)/shard_map/all_to_all | solution.py:42
  156.9 1.1 broadcast_in_dim.5
  158.0 8.2 %all-to-all-start.2 = ((f32[32,1,4224]{2,1,0:T(1,128)}), f32[32,1,4224]{2,1,0:T(1,128)S(1)}, u32[]{:S(2)}, u32[]{:S(2)}) async-start(f32[32,1,4224]{2,1,0:T(1,128)} %broadcast_in_dim.5), calls=%async_computation.4 | async-start | bytes 1081344 | tf_op jit(solution)/shard_map/all_to_all | solution.py:48
  166.2 0.0 reduce-scatter.5.cloned.1.call-start
  166.3 49.8 %reduce-scatter.3.cloned.1.call-done = bf16[4,64,1408]{2,1,0:T(8,128)(2,1)} async-done(((bf16[32,64,1408]{2,1,0:T(8,128)(2,1)}), bf16[4,64,1408]{2,1,0:T(8,128)(2,1)}) %reduce-scatter.3.cloned.1.call-update) | async-done | bytes 720912 | tf_op jit(solution)/shard_map/reduce_scatter | solution.py:63
  216.1 0.0 reduce-scatter.5.cloned.1.call-update
  216.1 0.2 reduce_sum.75
  216.3 0.0 all-to-all-done.2
  216.3 1.1 broadcast_in_dim.4
  217.4 4.8 %all-to-all-start.1 = ((bf16[8,32,2048]{2,1,0:T(8,128)(2,1)}), bf16[8,32,2048]{2,1,0:T(8,128)(2,1)S(1)}, u32[]{:S(2)}, u32[]{:S(2)}) async-start(bf16[8,32,2048]{2,1,0:T(8,128)(2,1)} %broadcast_in_dim.4), calls=%async_computation.1 | async-start | bytes 2097152 | tf_op jit(solution)/shard_map/all_to_all | solution.py:48
  222.2 0.9 copy.43
  223.1 0.3 reduce_sum.82
  223.4 0.1 fusion.24
  223.5 0.1 reshape.64
  223.5 0.1 reshape.63
  223.6 0.6 add.96
  224.2 0.6 add.95
  224.8 11.2 %all-to-all-done.1 = bf16[8,32,2048]{2,1,0:T(8,128)(2,1)S(1)} async-done(((bf16[8,32,2048]{2,1,0:T(8,128)(2,1)}), bf16[8,32,2048]{2,1,0:T(8,128)(2,1)S(1)}, u32[]{:S(2)}, u32[]{:S(2)}) %all-to-all-start.1) | async-done | bytes 1048608 | tf_op jit(solution)/shard_map/all_to_all | solution.py:48
  236.0 13.4 %reduce-scatter.5.cloned.1.call-done = bf16[1,64,1408]{2,1,0:T(8,128)(2,1)} async-done(((bf16[4,64,1408]{2,1,0:T(8,128)(2,1)}), bf16[1,64,1408]{2,1,0:T(8,128)(2,1)}) %reduce-scatter.5.cloned.1.call-update) | async-done | bytes 180240 | tf_op jit(solution)/shard_map/reduce_scatter | solution.py:63
  249.4 0.9 bitcast_convert_fusion
  250.4 0.8 slice_add_fusion
  251.2 1.0 copy.48
  (21 shorter events, 0.1 us)
Async XLA Ops:
  7.2 96.6 %all-gather.4.cloned.1.call-start = ((), (), s32[]{:S(2)}) async-start(), calls=%async_computation.7 | async-start | bytes 6488064 | tf_op jit(solution)/shard_map/all_gather | solution.py:24
  30.2 185.9 %reduce-scatter.3.cloned.1.call-start = ((), (), s32[]{:S(2)}) async-start(), calls=%async_computation.5 | async-start | bytes 6488064 | tf_op jit(solution)/shard_map/reduce_scatter | solution.py:63
  103.8 3.3 %copy-start.5 = (bf16[256,2048]{1,0:T(8,128)(2,1)S(1)}, bf16[256,2048]{1,0:T(8,128)(2,1)}, u32[]{:S(2)}) copy-start(bf16[256,2048]{1,0:T(8,128)(2,1)} %param.11) | copy-start | bytes 3145732
  103.8 3.3 %copy-start.6 = (bf16[256,2048]{1,0:T(8,128)(2,1)S(1)}, bf16[256,2048]{1,0:T(8,128)(2,1)}, u32[]{:S(2)}) copy-start(bf16[256,2048]{1,0:T(8,128)(2,1)} %param.12) | copy-start | bytes 3145732
  107.1 3.5 %copy-start = (bf16[4,8,64,1408]{3,2,1,0:T(8,128)(2,1)}, bf16[4,8,64,1408]{3,2,1,0:T(8,128)(2,1)S(1)}, u32[]{:S(2)}) copy-start(bf16[4,8,64,1408]{3,2,1,0:T(8,128)(2,1)S(1)} %copy.38) | copy-start | bytes 17301508
  138.3 18.7 %all-to-all-start = ((bf16[8,32,2048]{2,1,0:T(8,128)(2,1)}), bf16[8,32,2048]{2,1,0:T(8,128)(2,1)S(1)}, u32[]{:S(2)}, u32[]{:S(2)}) async-start(bf16[8,32,2048]{2,1,0:T(8,128)(2,1)} %bitcast.4), calls=%async_computation | async-start | bytes 2097152 | tf_op jit(solution)/shard_map/all_to_all | solution.py:42
  143.1 80.5 %copy-start.3 = (f32[3,704]{1,0:T(4,128)S(1)}, f32[3,704]{1,0:T(4,128)}, u32[]{:S(2)}) copy-start(f32[3,704]{1,0:T(4,128)} %param.21) | copy-start | bytes 25348
  143.2 81.0 %copy-start.4 = (f32[3,704]{1,0:T(4,128)S(1)}, f32[3,704]{1,0:T(4,128)}, u32[]{:S(2)}) copy-start(f32[3,704]{1,0:T(4,128)} %param.20) | copy-start | bytes 25348
  158.0 92.4 %copy-start.1 = (f32[64,704]{1,0:T(8,128)S(1)}, f32[64,704]{1,0:T(8,128)}, u32[]{:S(2)}) copy-start(f32[64,704]{1,0:T(8,128)} %param.19) | copy-start | bytes 540676
  158.0 92.4 %copy-start.2 = (f32[64,704]{1,0:T(8,128)S(1)}, f32[64,704]{1,0:T(8,128)}, u32[]{:S(2)}) copy-start(f32[64,704]{1,0:T(8,128)} %param.18) | copy-start | bytes 540676
  158.0 58.3 %all-to-all-start.2 = ((f32[32,1,4224]{2,1,0:T(1,128)}), f32[32,1,4224]{2,1,0:T(1,128)S(1)}, u32[]{:S(2)}, u32[]{:S(2)}) async-start(f32[32,1,4224]{2,1,0:T(1,128)} %broadcast_in_dim.5), calls=%async_computation.4 | async-start | bytes 1081344 | tf_op jit(solution)/shard_map/all_to_all | solution.py:48
  166.2 83.2 %reduce-scatter.5.cloned.1.call-start = ((), (), s32[]{:S(2)}) async-start(), calls=%async_computation.6 | async-start | bytes 901120 | tf_op jit(solution)/shard_map/reduce_scatter | solution.py:63
  217.4 18.7 %all-to-all-start.1 = ((bf16[8,32,2048]{2,1,0:T(8,128)(2,1)}), bf16[8,32,2048]{2,1,0:T(8,128)(2,1)S(1)}, u32[]{:S(2)}, u32[]{:S(2)}) async-start(bf16[8,32,2048]{2,1,0:T(8,128)(2,1)} %broadcast_in_dim.4), calls=%async_computation.1 | async-start | bytes 2097152 | tf_op jit(solution)/shard_map/all_to_all | solution.py:48
Sparse Core Ops, SparseCore 0:
  30.3 73.4 all-gather.3
  133.0 83.0 reduce-scatter.2
  218.9 30.4 reduce-scatter.4
where the time goes:
time: 259 us
  waiting for transfers between devices  159 us (61%)
  local copies, waits for them, and re-layouts  23.5 us (9%)
  blocking collectives  21.9 us (8%)
  starting transfers between devices  17.9 us (7%)
  between operations  13.9 us (5%)
  matrix products  13.3 us (5%)
  other arithmetic  9.24 us (4%)
    all_gather x1, waiting for transfers between devices, all_blocks(): pieces = lax.all_gather(pieces, axes[k])  71 us
    reduce_scatter x2, waiting for transfers between devices, reduced_to_own(): pieces = lax.psum_scatter(pieces, axes[k], scatter_dimension=0, tiled=True)  63.2 us
    all_gather x1, blocking collectives, all_blocks(): pieces = lax.all_gather(pieces, axes[k])  21.9 us
    all_to_all x1, waiting for transfers between devices, sent_and_summed(): pieces = lax.all_to_all(cut_along(array, dim, size), axis, 0, 0, tiled=True)  13.5 us
    all_to_all x2, starting transfers between devices, copy_for_each(): lax.all_to_all(jnp.broadcast_to(array[None], (size, *array.shape)), axis,...  13 us
    all_to_all x2, waiting for transfers between devices, copy_for_each(): lax.all_to_all(jnp.broadcast_to(array[None], (size, *array.shape)), axis,...  11.2 us
    convert_element_type x1, local copies, waits for them, and re-layouts, per_device(): summed = summed_rows((lax.dot_general(early_rows, both_grads, contract_fi...  8.36 us
    transpose x1, local copies, waits for them, and re-layouts, reduced_to_own(): pieces = jnp.moveaxis(pieces, order, range(len(axes))).reshape(-1, *inside)  5.75 us
  transfers between devices with their start and end apart: 6, of which 5 were waited for; matrix products, arithmetic and copies ran while one was open for 5% of the time, Pallas kernels for 0%

commit v1 on v0

v1 whole, which is shorter than its diff:
```python
import jax
import jax.numpy as jnp
from jax import lax
from jax.experimental import pallas as pl
from jax.experimental.pallas import tpu as pltpu
from jax.sharding import Mesh
from jax.sharding import PartitionSpec as P

FS = ("fs_0", "fs_1")
REP_FS = ("rep", "fs_0", "fs_1")
MESH = pl.DeviceIdType.MESH

NZ, NY, NT = 4, 8, 8
ROWS = 256
LANE = 128
CA, CB = 768, 640
WIDE = CA + CB
HALF = 704
F32, BF16 = jnp.float32, jnp.bfloat16
GELU_K = 0.7978845608028654
GELU_A = 0.044715


def al(v, m):
    return pl.multiple_of(v, m)


def low_lanes(shape):
    return lax.broadcasted_iota(jnp.int32, shape, 1) < 64


def swap_halves(v):
    return pltpu.roll(v, 64, 1)


def row_of(shape):
    return lax.broadcasted_iota(jnp.int32, shape, 0)


def later(v, by):
    return jnp.where(row_of(v.shape) >= by, pltpu.roll(v, by, 0), 0.0)


def sooner(v, by):
    n = v.shape[0]
    return jnp.where(row_of(v.shape) < n - by, pltpu.roll(v, n - by, 0), 0.0)


def gelu_parts(v):
    t = jnp.tanh(GELU_K * (v + GELU_A * v * v * v))
    return 0.5 * v * (1.0 + t), t


def gelu_slope(v, t):
    return 0.5 * (1.0 + t) + 0.5 * v * (1.0 - t * t) * GELU_K * (1.0 + 3.0 * GELU_A * v * v)


def kernel(
    late_ref,
    early_ref,
    cot_ref,
    w_ref,
    taps_ref,
    gsum_ref,
    usum_ref,
    gtsum_ref,
    utsum_ref,
    hid_ref,
    eg_ref,
    gnext_ref,
    unext_ref,
    gtnext_ref,
    utnext_ref,
    wa,
    wb,
    xp,
    xt,
    pre,
    cot,
    dpre,
    dpg,
    snd,
    rcv,
    fin,
    finr,
    dxp,
    dxr,
    egs,
    tsum,
    tzr,
    tys,
    tyr,
    tfr,
    ssem,
    rsem,
):
    rep = lax.axis_index("rep")
    z = lax.axis_index("fs_0")
    y = lax.axis_index("fs_1")
    t = lax.axis_index("tp")
    scale = (NZ * NY * ROWS) ** -0.5

    def ring(k):
        g = lax.rem(rep * NZ + z + 2 * NZ + k, 2 * NZ)
        return {"rep": lax.div(g, NZ), "fs_0": lax.rem(g, NZ)}

    def zdev(k):
        return {"fs_0": lax.rem(z + NZ + k, NZ)}

    def ydev(k):
        return {"fs_1": lax.rem(y + NY + k, NY)}

    def tdev(k):
        return {"tp": lax.rem(t + NT + k, NT)}

    def zat(k):
        return lax.rem(z + NZ + k, NZ)

    def yat(k):
        return lax.rem(y + NY + k, NY)

    peers = [ring(1), ring(-1), ring(2), ring(-2)]
    peers += [zdev(k) for k in range(1, NZ)]
    peers += [ydev(k) for k in range(1, NY)]
    peers += [tdev(k) for k in range(1, NT)]

    barrier = pltpu.get_barrier_semaphore()
    for dev in peers:
        pl.semaphore_signal(barrier, inc=1, device_id=dev, device_id_type=MESH)
    pl.semaphore_wait(barrier, len(peers))

    slots = {}
    sent = []

    def slot(name):
        return slots.setdefault(name, len(slots))

    def copy_of(name, src, dst, dev):
        k = slot(name)
        return pltpu.make_async_remote_copy(
            src_ref=src,
            dst_ref=dst,
            send_sem=ssem.at[k],
            recv_sem=rsem.at[k],
            device_id=dev,
            device_id_type=MESH,
        )

    def send(name, src, dst, dev):
        c = copy_of(name, src, dst, dev)
        c.start()
        sent.append(c)

    def got(name, dst):
        copy_of(name, dst, dst, ydev(1)).wait_recv()

    def wrow(zz, first, n):
        return pl.ds(al(zz * 64 + first, 32), n)

    own = wrow(z, 0, 64)

    a_src = w_ref.at[:, pl.ds(0, CA)]
    send(("a1", 1), a_src, wa.at[y, own], ring(1))
    send(("a1", -1), a_src, wa.at[y, own], ring(-1))
    for h, d in ((0, 1), (1, -1)):
        send(
            ("b1", d, 0, h),
            w_ref.at[pl.ds(32 * h, 32), pl.ds(CA, CB)],
            wb.at[y, wrow(z, 32 * h, 32)],
            ydev(d),
        )
        send(
            ("b1", d, 0, 1 - h),
            w_ref.at[pl.ds(32 * (1 - h), 32), pl.ds(CA, CB)],
            wb.at[y, wrow(z, 32 * (1 - h), 32)],
            ydev(d),
        )
    send(("a1", 2), w_ref.at[pl.ds(0, 32), pl.ds(0, CA)], wa.at[y, wrow(z, 0, 32)], ring(2))
    send(("a1", -2), w_ref.at[pl.ds(32, 32), pl.ds(0, CA)], wa.at[y, wrow(z, 32, 32)], ring(-2))
    b_src = w_ref.at[:, pl.ds(CA, CB)]
    send(("b2", 0, 1), b_src, wb.at[y, own], ring(1))
    send(("b2", 0, -1), b_src, wb.at[y, own], ring(-1))

    wa[y, own, :] = w_ref[:, 0:CA]
    wb[y, own, :] = w_ref[:, CA:WIDE]

    def order_rows(src_ref, first):
        def one(yp, carry):
            for zp in range(2):
                a = src_ref[:, pl.ds(al(2 * zp * 512 + yp * LANE, LANE), LANE)].astype(F32)
                b = src_ref[:, pl.ds(al((2 * zp + 1) * 512 + yp * LANE, LANE), LANE)].astype(F32)
                low = low_lanes(a.shape)
                cols = slice(zp * LANE, (zp + 1) * LANE)
                xp[2 * yp, first : first + ROWS, cols] = jnp.where(low, a, swap_halves(b)).astype(BF16)
                xp[2 * yp + 1, first : first + ROWS, cols] = jnp.where(low, swap_halves(a), b).astype(BF16)
            return carry

        lax.fori_loop(0, NY // 2, one, 0)

    order_rows(early_ref, ROWS)

    def turn(yb, carry):
        xt[yb, 0] = xp[yb, ROWS : 2 * ROWS, :].astype(F32).T.astype(BF16)
        return carry

    lax.fori_loop(0, NY, turn, 0)
    for k in range(1, NZ):
        send(("xz", k), xt.at[t, 0], xt.at[t, k], zdev(-k))

    def a1_take():
        for k in (1, -1):
            got(("a1", k), wa.at[y, wrow(zat(-k), 0, 64)])
        got(("a1", 2), wa.at[y, wrow(zat(2), 0, 32)])
        got(("a1", -2), wa.at[y, wrow(zat(2), 32, 32)])
        for q in range(NZ):
            for d in (1, -1):
                blk = wa.at[y, pl.ds(64 * q, 64)]
                send(("a2", d, 0, q), blk, blk, ydev(d))

    def a2_last(d):
        return (0, 1) if d == 1 else (2, 3)

    def a2_take(s, qs):
        for q in qs:
            for d in (1, -1):
                if s == 4 and q not in a2_last(d):
                    continue
                blk = wa.at[yat(-d * s), pl.ds(64 * q, 64)]
                got(("a2", d, s - 1, q), blk)
                if s < 3 or (s == 3 and q in a2_last(d)):
                    send(("a2", d, s, q), blk, blk, ydev(d))

    def b1_take(s):
        for d in (1, -1):
            mine = 0 if d == 1 else 1
            for h in (mine, 1 - mine):
                if s == 4 and h != mine:
                    continue
                blk = wb.at[yat(-d * s), wrow(z, 32 * h, 32)]
                got(("b1", d, s - 1, h), blk)
                if s < 3 or (s == 3 and h == mine):
                    send(("b1", d, s, h), blk, blk, ydev(d))
        for e in ordinals(s):
            blk = wb.at[yat(-e), own]
            for k in (1, -1):
                send(("b2", e, k), blk, blk, ring(k))

    def ordinals(s):
        return (0,) if s == 0 else ((4,) if s == 4 else (s, -s))

    def b2_take(s):
        for e in ordinals(s):
            for k in (1, -1):
                yb = yat(-e)
                got(("b2", e, k), wb.at[yb, wrow(zat(-k), 0, 64)])
                half = wb.at[yb, wrow(zat(-k), 0 if k == 1 else 32, 32)]
                send(("b2f", e, k), half, half, ring(k))

    def b2f_take(s):
        for e in ordinals(s):
            yb = yat(-e)
            got(("b2f", e, 1), wb.at[yb, wrow(zat(2), 0, 32)])
            got(("b2f", e, -1), wb.at[yb, wrow(zat(2), 32, 32)])

    def project(w, first, width, yb, start):
        rows = xp[yb]

        def tile(c0, n):
            cols = pl.ds(first + c0, n)
            part = jnp.dot(rows, w[yb, :, pl.ds(c0, n)], preferred_element_type=F32)
            pre[:, cols] = part if start else pre[:, cols] + part

        def one(c, carry):
            tile(al(c * 256, 256), 256)
            return carry

        lax.fori_loop(0, width // 256, one, 0)
        if width % 256:
            tile(width - width % 256, width % 256)

    def project_a(s):
        for e in ordinals(s):
            project(wa, 0, CA, yat(-e), s == 0)

    def project_b(s):
        for e in ordinals(s):
            project(wb, CA, CB, yat(-e), s == 0)

    b1_take(1)
    a1_take()
    b2_take(0)
    order_rows(late_ref, 0)
    b1_take(2)
    b2_take(1)
    project_a(0)
    a2_take(1, (0, 1))
    b1_take(3)
    a2_take(1, (2, 3))
    b2_take(2)
    b1_take(4)
    for k in range(1, NZ):
        got(("xz", k), xt.at[t, k])
    mine = xt.at[t, pl.ds(1, 3)]
    for k in (2, 4, 6):
        send(("xx", k), mine, mine, tdev(k))
    pair = {"tp": t + 1 - 2 * lax.rem(t, 2)}
    send(("xc", 0), mine, mine, pair)
    project_a(1)
    a2_take(2, (0, 1))
    b2_take(3)
    a2_take(2, (2, 3))
    b2f_take(0)
    b2f_take(1)
    b2_take(4)
    project_a(2)
    project_b(0)
    a2_take(3, (0, 1))
    a2_take(3, (2, 3))
    project_b(1)
    project_a(3)
    b2f_take(2)
    project_b(2)
    cot[:, 640:CA] = jnp.zeros((ROWS, LANE), BF16)
    cot[:, 0:HALF] = cot_ref[...]
    b2f_take(3)
    project_b(3)
    b2f_take(4)
    project_b(4)
    a2_take(4, range(NZ))
    project_a(4)

    def tap(cols):
        return [taps_ref[j : j + 1, cols] for j in range(3)]

    def mixed(first, cols):
        v = pre[first : first + ROWS, cols].astype(BF16).astype(F32)
        w = tap(cols)
        return v, w[0] * later(v, 2) + w[1] * later(v, 1) + w[2] * v, w

    def back(d, v, w, cols, n):
        dpre[:, cols] = (w[2] * d + w[1] * sooner(d, 1) + w[0] * sooner(d, 2)).astype(BF16)
        q, r = lax.div(n, 3), lax.rem(n, 3)
        spot = pl.ds(al(r * LANE, LANE), LANE)
        for j, u in enumerate((later(v, 2), later(v, 1), v)):
            tsum[q, j : j + 1, spot] = jnp.sum(d * u, axis=0, keepdims=True) * scale

    def tile_cols(n):
        return pl.ds(al(n * LANE, LANE), LANE)

    tsum[...] = jnp.zeros_like(tsum)
    dpre[:, WIDE:] = jnp.zeros((ROWS, LANE), BF16)

    def early_tile(n, carry):
        gc, uc = tile_cols(n), tile_cols(n + 5)
        gv, gm, gw = mixed(ROWS, gc)
        uv, um, uw = mixed(ROWS, uc)
        c = cot[:, gc].astype(F32)
        act, th = gelu_parts(gm)
        back(c * um * gelu_slope(gm, th), gv, gw, gc, n)
        back(c * act, uv, uw, uc, n + 5)
        return carry

    lax.fori_loop(0, 5, early_tile, 0)
    last = slice(1280, 1408)
    mv, mm, mw = mixed(ROWS, last)
    c = cot[:, 640:CA].astype(F32)
    act, th = gelu_parts(mm)
    dg = c * swap_halves(mm) * gelu_slope(mm, th)
    du = swap_halves(c * act)
    back(jnp.where(low_lanes(dg.shape), dg, du), mv, mw, last, 10)

    for i in range(3):
        for k in range(1, NZ):
            send(
                ("dp", i, k),
                dpre.at[:, pl.ds(al((zat(-k) * 3 + i) * LANE, LANE), LANE)],
                dpg.at[i, k],
                zdev(-k),
            )
    for k in range(1, NZ):
        send(("tz", k), tsum.at[zat(-k)], tzr.at[k], zdev(-k))
    for i in range(3):
        dpg[i, 0] = dpre[:, pl.ds(al((z * 3 + i) * LANE, LANE), LANE)]

    def dx(yb, carry):
        nt = (((1,), (1,)), ((), ()))
        v = lax.dot_general(dpre[:, 0:CA], wa[yb], nt, preferred_element_type=F32)
        v = v + lax.dot_general(dpre[:, CA:WIDE], wb[yb], nt, preferred_element_type=F32)
        dxp[:, pl.ds(al(yb * 256, 256), 256)] = v.astype(BF16)
        return carry

    lax.fori_loop(0, NY, dx, 0)

    def strip(tt):
        return pl.ds(al(tt * 32, 32), 32)

    for k in range(1, NT):
        to = lax.rem(t + NT - k, NT)
        send(("dx", k), dxp.at[strip(to)], dxr.at[k], tdev(-k))

    for k in (2, 4, 6):
        row = lax.rem(t + NT - k, NT)
        blk = xt.at[row, pl.ds(1, 3)]
        got(("xx", k), blk)
        send(("xc", k), blk, blk, pair)

    for k in range(1, NZ):
        got(("tz", k), tzr.at[k])
    tys[...] = tsum[z] + tzr[1] + tzr[2] + tzr[3]
    for k in range(1, NY):
        send(("ty", k), tys, tyr.at[k], ydev(-k))

    for k in (0, 2, 4, 6):
        row = lax.rem(t + 1 - 2 * lax.rem(t, 2) + NT - k, NT)
        got(("xc", k), xt.at[row, pl.ds(1, 3)])

    def term(i, yb):
        v = jnp.dot(xt[yb, 0], dpg[i, 0], preferred_element_type=F32)
        for k in range(1, NZ):
            v = v + jnp.dot(xt[yb, k], dpg[i, k], preferred_element_type=F32)
        return v * scale

    def side(d):
        return 0 if d == 1 else 1

    def part(d):
        return pl.ds(0, 128) if d == 1 else pl.ds(128, 128)

    def rs(i, s):
        if s == 0:
            for k in range(1, NZ):
                got(("dp", i, k), dpg.at[i, k])
            v = term(i, yat(4))
            for d in (1, -1):
                buf = snd.at[side(d), i, 0, part(d)]
                buf[...] = (v[0:128] if d == 1 else v[128:256]).astype(BF16)
                send(("rs", i, 0, d), buf, rcv.at[side(d), i, 0, part(d)], ydev(d))
            return
        if s < 4:
            for d in (1, -1):
                snd_f = term(i, yat(d * (4 - s)))
                buf = snd.at[side(d), i, s]
                if s == 1:
                    got(("rs", i, 0, d), rcv.at[side(d), i, 0, part(d)])
                    in_ = rcv[side(d), i, 0, part(d), :].astype(F32)
                    if d == 1:
                        buf[0:128, :] = (snd_f[0:128] + in_).astype(BF16)
                        buf[128:256, :] = snd_f[128:256].astype(BF16)
                    else:
                        buf[0:128, :] = snd_f[0:128].astype(BF16)
                        buf[128:256, :] = (snd_f[128:256] + in_).astype(BF16)
                else:
                    got(("rs", i, s - 1, d), rcv.at[side(d), i, s - 1])
                    buf[...] = (snd_f + rcv[side(d), i, s - 1].astype(F32)).astype(BF16)
                send(("rs", i, s, d), buf, rcv.at[side(d), i, s], ydev(d))
            return
        v = term(i, y)
        for d in (1, -1):
            got(("rs", i, 3, d), rcv.at[side(d), i, 3])
            v = v + rcv[side(d), i, 3].astype(F32)
        fin[i] = v.astype(BF16)
        for k in range(1, NZ):
            send(("fin", i, k), fin.at[i, wrow(zat(-k), 0, 64)], finr.at[k, i], zdev(-k))
        finr[0, i] = fin[i, own, :]

    def dx_reduce():
        for k in range(1, NT):
            got(("dx", k), dxr.at[k])
        v = dxp[strip(t), :].astype(F32)
        for k in range(1, NT):
            v = v + dxr[k].astype(F32)
        for yp in range(NY // 2):
            for zp in range(2):
                a = v[:, 2 * yp * 256 + zp * LANE : 2 * yp * 256 + (zp + 1) * LANE]
                b = v[:, (2 * yp + 1) * 256 + zp * LANE : (2 * yp + 1) * 256 + (zp + 1) * LANE]
                low = low_lanes(a.shape)
                at0 = 2 * zp * 512 + yp * LANE
                egs[:, at0 : at0 + LANE] = jnp.where(low, a, swap_halves(b)).astype(BF16)
                egs[:, at0 + 512 : at0 + 512 + LANE] = jnp.where(low, swap_halves(a), b).astype(BF16)
        for k in range(1, NT):
            send(("eg", k), egs, eg_ref.at[strip(t)], tdev(-k))
        eg_ref[strip(t), :] = egs[...]

    def taps_finish():
        v = tys[...]
        for k in range(1, NY):
            got(("ty", k), tyr.at[k])
            v = v + tyr[k]
        tfr[0] = v
        for k in range(1, NZ):
            send(("tf", k), tfr.at[0], tfr.at[k], zdev(-k))

    def late_tile(n, carry):
        gc = tile_cols(n)
        _, gm, _ = mixed(0, gc)
        _, um, _ = mixed(0, tile_cols(n + 5))
        act, _ = gelu_parts(gm)
        hid_ref[:, gc] = (act * um).astype(BF16)
        return carry

    rs(0, 0)
    lax.fori_loop(0, 5, late_tile, 0)
    _, mm, _ = mixed(0, last)
    act, _ = gelu_parts(mm)
    hid_ref[:, 640:HALF] = (act * swap_halves(mm)).astype(BF16)[:, 0:64]
    rs(0, 1)
    rs(1, 0)
    rs(0, 2)
    rs(1, 1)
    dx_reduce()
    rs(0, 3)
    rs(2, 0)
    rs(1, 2)
    taps_finish()
    rs(2, 1)
    rs(0, 4)
    rs(1, 3)
    rs(2, 2)
    rs(1, 4)
    rs(2, 3)
    rs(2, 4)

    def tile_out(n, v):
        if n < 5:
            cols = slice(n * LANE, (n + 1) * LANE)
            gnext_ref[:, cols] = gsum_ref[:, cols] + v
        elif n < 10:
            cols = slice((n - 5) * LANE, (n - 4) * LANE)
            unext_ref[:, cols] = usum_ref[:, cols] + v
        else:
            gnext_ref[:, 640:HALF] = gsum_ref[:, 640:HALF] + v[:, 0:64]
            unext_ref[:, 640:HALF] = usum_ref[:, 640:HALF] + swap_halves(v)[:, 0:64]

    def taps_out(n, v):
        if n < 5:
            cols = slice(n * LANE, (n + 1) * LANE)
            gtnext_ref[:, cols] = gtsum_ref[:, cols] + v[0:3]
        elif n < 10:
            cols = slice((n - 5) * LANE, (n - 4) * LANE)
            utnext_ref[:, cols] = utsum_ref[:, cols] + v[0:3]
        else:
            gtnext_ref[:, 640:HALF] = gtsum_ref[:, 640:HALF] + v[0:3, 0:64]
            utnext_ref[:, 640:HALF] = utsum_ref[:, 640:HALF] + swap_halves(v)[0:3, 0:64]

    for k in range(1, NZ):
        got(("tf", k), tfr.at[k])
    for k in range(1, NT):
        got(("eg", k), eg_ref.at[strip(lax.rem(t + k, NT))])
    for i in range(3):
        for k in range(1, NZ):
            got(("fin", i, k), finr.at[k, i])
    for n in range(11):
        k = lax.rem(n // 3 + NZ - z, NZ)
        tile_out(n, finr[k, n % 3].astype(F32))
        v = tfr[k]
        taps_out(n, v[:, (n % 3) * LANE : (n % 3 + 1) * LANE])
    for c in sent:
        c.wait_send()


def per_device(
    late_rows,
    early_rows,
    hidden_cot,
    gate_weight,
    up_weight,
    gate_taps,
    up_taps,
    gate_grad_sum,
    up_grad_sum,
    gate_taps_sum,
    up_taps_sum,
):
    def joined(g, u):
        return jnp.concatenate([g[:, :640], u[:, :640], g[:, 640:], u[:, 640:]], axis=1)

    weight = joined(gate_weight, up_weight)
    taps = joined(gate_taps, up_taps).astype(F32)
    vmem = pl.BlockSpec(memory_space=pltpu.VMEM)
    shapes = (
        ((ROWS, HALF), BF16),
        ((ROWS, 2048), BF16),
        ((64, HALF), F32),
        ((64, HALF), F32),
        ((3, HALF), F32),
        ((3, HALF), F32),
    )
    n_sem = 170
    return pl.pallas_call(
        kernel,
        out_shape=[jax.ShapeDtypeStruct(s, d) for s, d in shapes],
        in_specs=[vmem] * 9,
        out_specs=[vmem] * 6,
        scratch_shapes=[
            pltpu.VMEM((NY, 256, CA), BF16),
            pltpu.VMEM((NY, 256, CB), BF16),
            pltpu.VMEM((NY, 2 * ROWS, 256), BF16),
            pltpu.VMEM((NY, NZ, 256, ROWS), BF16),
            pltpu.VMEM((2 * ROWS, WIDE), F32),
            pltpu.VMEM((ROWS, CA), BF16),
            pltpu.VMEM((ROWS, WIDE + LANE), BF16),
            pltpu.VMEM((3, NZ, ROWS, LANE), BF16),
            pltpu.VMEM((2, 3, 4, 256, LANE), BF16),
            pltpu.VMEM((2, 3, 4, 256, LANE), BF16),
            pltpu.VMEM((3, 256, LANE), BF16),
            pltpu.VMEM((NZ, 3, 64, LANE), BF16),
            pltpu.VMEM((ROWS, 2048), BF16),
            pltpu.VMEM((NT, 32, 2048), BF16),
            pltpu.VMEM((32, 2048), BF16),
            pltpu.VMEM((NZ, 8, 384), F32),
            pltpu.VMEM((NZ, 8, 384), F32),
            pltpu.VMEM((8, 384), F32),
            pltpu.VMEM((NY, 8, 384), F32),
            pltpu.VMEM((NZ, 8, 384), F32),
            pltpu.SemaphoreType.DMA((n_sem,)),
            pltpu.SemaphoreType.DMA((n_sem,)),
        ],
        compiler_params=pltpu.CompilerParams(
            collective_id=0, has_side_effects=True, vmem_limit_bytes=60 * 1024 * 1024
        ),
    )(
        late_rows,
        early_rows,
        hidden_cot,
        weight,
        taps,
        gate_grad_sum,
        up_grad_sum,
        gate_taps_sum,
        up_taps_sum,
    )


def solution(mesh):
    split = Mesh(
        mesh.devices.reshape(mesh.shape["rep"], NZ, NY, mesh.shape["tp"]),
        ("rep", "fs_0", "fs_1", "tp"),
    )
    placed = (
        P(REP_FS, None),
        P(REP_FS, None),
        P(REP_FS, "tp"),
        P(FS, "tp"),
        P(FS, "tp"),
        P(None, "tp"),
        P(None, "tp"),
        P(REP_FS, "tp"),
        P(REP_FS, "tp"),
        P("rep", "tp"),
        P("rep", "tp"),
    )
    return jax.shard_map(
        per_device,
        mesh=split,
        in_specs=placed,
        out_specs=(
            P(REP_FS, "tp"),
            P(REP_FS, None),
            P(REP_FS, "tp"),
            P(REP_FS, "tp"),
            P("rep", "tp"),
            P("rep", "tp"),
        ),
        check_vma=False,
    )
```

time: 259 us -> 131 us (0.51)
  waiting for transfers between devices: 159 us -> 0 us
  Pallas kernels: 0 us -> 117 us
  blocking collectives: 21.9 us -> 0 us
  starting transfers between devices: 17.9 us -> 0 us
  matrix products: 13.3 us -> 0 us
  between operations: 13.9 us -> 0.7 us
  local copies, waits for them, and re-layouts: 23.5 us -> 10.7 us
  other arithmetic: 9.24 us -> 0.61 us
    pallas_call x0 -> x1, Pallas kernels: none -> 117 us  [per_device(): pl.pallas_call(kernel, out_shape=[jax.ShapeDtypeStruct(s, d) for s, d in...]
    all_gather x1 -> x0, waiting for transfers between devices: 71 us -> none  [all_blocks(): pieces = lax.all_gather(pieces, axes[k])]
    reduce_scatter x2 -> x0, waiting for transfers between devices: 63.2 us -> none  [reduced_to_own(): pieces = lax.psum_scatter(pieces, axes[k], scatter_dimension=0, tiled=True)]
    all_to_all x3 -> x0, waiting for transfers between devices: 24.7 us -> none  [the longest x1 13.5 us: sent_and_summed(): pieces = lax.all_to_all(cut_along(array, dim, size), axis, 0, 0, tiled=True)]
    all_gather x1 -> x0, blocking collectives: 21.9 us -> none  [all_blocks(): pieces = lax.all_gather(pieces, axes[k])]
    all_to_all x3 -> x0, starting transfers between devices: 17.8 us -> none  [the longest x2 13 us: copy_for_each(): lax.all_to_all(jnp.broadcast_to(array[None], (size, *array.shape)), axis,...]
    dot_general x3 -> x0, matrix products: 13.3 us -> none  [the longest x1 5.43 us: per_device(): lax.dot_general(both_grads, whole_joined, contract_last, preferred_elemen...]
    transpose x2 -> x0, local copies, waits for them, and re-layouts: 9.05 us -> none  [the longest x1 5.75 us: reduced_to_own(): pieces = jnp.moveaxis(pieces, order, range(len(axes))).reshape(-1, *inside)]
  transfers between devices with their start and end apart: 6 -> 0, of which waited for: 5 -> 0; matrix products, arithmetic and copies ran while one was open for 5% -> 0% of each run, Pallas kernels for 0% -> 0%
where the time goes in v1:
time: 131 us; the launch traced here: 129 us
  Pallas kernels  117 us (89%)
  local copies, waits for them, and re-layouts  10.7 us (8%)
    pallas_call x1, Pallas kernels, per_device(): pl.pallas_call(kernel, out_shape=[jax.ShapeDtypeStruct(s, d) for s, d in...  117 us
    unnamed x16, local copies, waits for them, and re-layouts  6.28 us

profile of v1, /device:TPU:6, one launch (start us, length us, event | category | flops | bytes accessed | tf_op | source)
XLA Modules:
  0.0 129.2 jit_solution(5125648361691912034)
XLA Ops:
  0.6 0.0 slice-start.7
  0.6 0.0 slice-start.4
  0.7 0.0 slice-start.5
  0.7 0.0 slice-start.6
  0.7 0.6 slice-done.7
  1.3 0.0 slice-done.4
  1.3 0.0 slice-done.5
  1.4 0.0 slice-done.6
  1.4 0.1 concatenate.7
  1.5 0.6 convert_element_type.3.taps_ref
  2.1 0.0 slice-start
  2.1 0.0 slice-start.1
  2.1 0.0 slice-start.2
  2.1 0.0 slice-start.3
  2.1 0.0 copy-start
  2.1 0.7 slice-done
  2.8 0.2 slice-done.1
  3.0 0.0 slice-done.2
  3.0 0.1 slice-done.3
  3.0 0.8 concatenate.6.w_ref
  3.8 0.0 copy-done
  3.8 0.9 copy.17.cot_ref
  4.7 117.2 %shard_map.154 = (bf16[256,704]{1,0:T(8,128)(2,1)}, bf16[256,2048]{1,0:T(8,128)(2,1)}, f32[64,704]{1,0:T(8,128)}, f32[64,704]{1,0:T(8,128)}, f32[3,704]{1,0:T(4,128)}, /*index=5*/f32[3,704]{1,0:T(4,128)}) custom-call(bf16[256,2048]{1,0:T(8,128)(2,1)} %late_ref.1, bf16[256,2048]{1,0:T(8,128)(2,1)} %early_ref.1, bf16[256,704]{1,0:T(8,128)(2,1)} %copy.17.cot_ref, ...), custom_call_target="tpu_custom_call" | custom-call | tf_op jit(solution)/shard_map/pallas_call | solution.py:589
  121.9 1.9 %copy.18 = bf16[256,704]{0,1:T(8,128)(2,1)} copy(bf16[256,704]{1,0:T(8,128)(2,1)} %get-tuple-element.6) | data formatting | bytes 720896 | tf_op jit(solution)/shard_map/pallas_call | solution.py:589
  123.8 0.0 copy-start.2
  123.8 2.3 %copy.24 = bf16[256,2048]{1,0:T(8,128)(2,1)} copy(bf16[256,2048]{1,0:T(8,128)(2,1)} %get-tuple-element.19) | data formatting | bytes 2097152
  126.2 0.0 copy-done.2
  126.2 0.0 copy-start.1
  126.2 0.7 copy.25
  126.8 0.3 copy-done.1
  127.2 0.0 copy-start.4
  127.2 0.7 copy.26
  127.8 0.0 copy-done.4
  127.9 0.0 copy-start.3
  127.9 0.6 copy.27
  128.5 0.1 copy-done.3
  128.6 0.6 copy.28
Async XLA Ops:
  0.6 0.7 slice-start.7
  0.6 0.7 slice-start.4
  0.7 0.7 slice-start.5
  0.7 0.7 slice-start.6
  2.1 0.7 slice-start
  2.1 0.9 slice-start.1
  2.1 0.9 slice-start.2
  2.1 1.0 slice-start.3
  2.1 1.7 %copy-start = (bf16[256,704]{0,1:T(8,128)(2,1)S(1)}, bf16[256,704]{0,1:T(8,128)(2,1)}, u32[]{:S(2)}) copy-start(bf16[256,704]{0,1:T(8,128)(2,1)} %param.13) | copy-start | bytes 1081348
  123.8 2.3 %copy-start.2 = (f32[64,704]{1,0:T(8,128)S(1)}, f32[64,704]{1,0:T(8,128)}, u32[]{:S(2)}) copy-start(f32[64,704]{1,0:T(8,128)} %get-tuple-element.20) | copy-start | bytes 540676
  126.2 1.0 copy-start.1
  127.2 0.7 copy-start.4
  127.9 0.7 copy-start.3

commit v2 on v1

--- a/solution.py
+++ b/solution.py
@@ -13,9 +13,10 @@
 NZ, NY, NT = 4, 8, 8
 ROWS = 256
 LANE = 128
-CA, CB = 768, 640
+CA, CB = 896, 512
 WIDE = CA + CB
 HALF = 704
+GPOS, UPOS = (0, 1, 2, 7, 9), (3, 4, 5, 8, 10)
 F32, BF16 = jnp.float32, jnp.bfloat16
 GELU_K = 0.7978845608028654
 GELU_A = 0.044715
@@ -56,13 +57,15 @@
 
 
 def kernel(
-    late_ref,
-    early_ref,
-    cot_ref,
-    w_ref,
-    taps_ref,
-    gsum_ref,
-    usum_ref,
+    late_hbm,
+    early_hbm,
+    cot_hbm,
+    gw_hbm,
+    uw_hbm,
+    gsum_hbm,
+    usum_hbm,
+    gt_ref,
+    ut_ref,
     gtsum_ref,
     utsum_ref,
     hid_ref,
@@ -71,13 +74,25 @@
     unext_ref,
     gtnext_ref,
     utnext_ref,
+    late_ref,
+    early_ref,
+    cot_ref,
+    gw,
+    uw,
+    gsum_ref,
+    usum_ref,
+    wmix,
+    taps_ref,
     wa,
     wb,
-    xp,
+    xe,
+    xl,
     xt,
     pre,
+    prel,
     cot,
     dpre,
+    dpq,
     dpg,
     snd,
     rcv,
@@ -91,6 +106,7 @@
     tys,
     tyr,
     tfr,
+    lsem,
     ssem,
     rsem,
 ):
@@ -127,7 +143,22 @@
     barrier = pltpu.get_barrier_semaphore()
     for dev in peers:
         pl.semaphore_signal(barrier, inc=1, device_id=dev, device_id_type=MESH)
-    pl.semaphore_wait(barrier, len(peers))
+
+    pulls = []
+    for n, (src, dst) in enumerate(
+        (
+            (gw_hbm, gw),
+            (uw_hbm, uw),
+            (early_hbm, early_ref),
+            (late_hbm, late_ref),
+            (cot_hbm, cot_ref),
+            (gsum_hbm, gsum_ref),
+            (usum_hbm, usum_ref),
+        )
+    ):
+        c = pltpu.make_async_copy(src, dst, lsem.at[n])
+        c.start()
+        pulls.append(c)
 
     slots = {}
     sent = []
@@ -159,63 +190,110 @@
 
     own = wrow(z, 0, 64)
 
-    a_src = w_ref.at[:, pl.ds(0, CA)]
-    send(("a1", 1), a_src, wa.at[y, own], ring(1))
-    send(("a1", -1), a_src, wa.at[y, own], ring(-1))
-    for h, d in ((0, 1), (1, -1)):
-        send(
-            ("b1", d, 0, h),
-            w_ref.at[pl.ds(32 * h, 32), pl.ds(CA, CB)],
-            wb.at[y, wrow(z, 32 * h, 32)],
-            ydev(d),
-        )
-        send(
-            ("b1", d, 0, 1 - h),
-            w_ref.at[pl.ds(32 * (1 - h), 32), pl.ds(CA, CB)],
-            wb.at[y, wrow(z, 32 * (1 - h), 32)],
-            ydev(d),
-        )
-    send(("a1", 2), w_ref.at[pl.ds(0, 32), pl.ds(0, CA)], wa.at[y, wrow(z, 0, 32)], ring(2))
-    send(("a1", -2), w_ref.at[pl.ds(32, 32), pl.ds(0, CA)], wa.at[y, wrow(z, 32, 32)], ring(-2))
-    b_src = w_ref.at[:, pl.ds(CA, CB)]
-    send(("b2", 0, 1), b_src, wb.at[y, own], ring(1))
-    send(("b2", 0, -1), b_src, wb.at[y, own], ring(-1))
-
-    wa[y, own, :] = w_ref[:, 0:CA]
-    wb[y, own, :] = w_ref[:, CA:WIDE]
-
-    def order_rows(src_ref, first):
+    pulls[0].wait()
+    pulls[1].wait()
+    wmix[:, 0:64] = gw[:, 640:HALF].astype(F32)
+    wmix[:, 64:LANE] = uw[:, 640:HALF].astype(F32)
+    taps_ref[0:3, 768:832] = gt_ref[:, 640:HALF].astype(F32)
+    taps_ref[0:3, 832:CA] = ut_ref[:, 640:HALF].astype(F32)
+    wa[y, own, 768:CA] = wmix[...].astype(BF16)
+    for n in range(5):
+        cols = slice(n * LANE, (n + 1) * LANE)
+        for src, tsrc, pos in ((gw, gt_ref, GPOS[n]), (uw, ut_ref, UPOS[n])):
+            here = slice(pos * LANE, (pos + 1) * LANE)
+            taps_ref[0:3, here] = tsrc[:, cols].astype(F32)
+            if pos < 7:
+                wa[y, own, here] = src[:, cols]
+            else:
+                wb[y, own, (pos - 7) * LANE : (pos - 6) * LANE] = src[:, cols]
+    pl.semaphore_wait(barrier, len(peers))
+
+    def zrow(q):
+        return zat((0, -1, 1, 2)[q])
+
+    def a2_own(q):
+        blk = wa.at[y, wrow(zrow(q), 0, 64)]
+        for d in (1, -1):
+            send(("a2", d, 0, q), blk, blk, ydev(d))
+
+    a_own, b_own = wa.at[y, own], wb.at[y, own]
+    for k in (1, -1):
+        send(("a1", k), a_own, a_own, ring(k))
+    for h, d in ((0, 1), (1, -1), (1, 1), (0, -1)):
+        blk = wb.at[y, wrow(z, 32 * h, 32)]
+        send(("b1", d, 0, h), blk, blk, ydev(d))
+    for h, k in ((0, 2), (1, -2)):
+        blk = wa.at[y, wrow(z, 32 * h, 32)]
+        send(("a1", k), blk, blk, ring(k))
+    a2_own(0)
+    for k in (1, -1):
+        send(("b2", 0, k), b_own, b_own, ring(k))
+
+    def order_rows(src_ref, dst):
         def one(yp, carry):
             for zp in range(2):
                 a = src_ref[:, pl.ds(al(2 * zp * 512 + yp * LANE, LANE), LANE)].astype(F32)
                 b = src_ref[:, pl.ds(al((2 * zp + 1) * 512 + yp * LANE, LANE), LANE)].astype(F32)
                 low = low_lanes(a.shape)
                 cols = slice(zp * LANE, (zp + 1) * LANE)
-                xp[2 * yp, first : first + ROWS, cols] = jnp.where(low, a, swap_halves(b)).astype(BF16)
-                xp[2 * yp + 1, first : first + ROWS, cols] = jnp.where(low, swap_halves(a), b).astype(BF16)
+                dst[2 * yp, :, cols] = jnp.where(low, a, swap_halves(b)).astype(BF16)
+                dst[2 * yp + 1, :, cols] = jnp.where(low, swap_halves(a), b).astype(BF16)
             return carry
 
         lax.fori_loop(0, NY // 2, one, 0)
 
-    order_rows(early_ref, ROWS)
+    pulls[2].wait()
+    order_rows(early_ref, xe)
 
     def turn(yb, carry):
-        xt[yb, 0] = xp[yb, ROWS : 2 * ROWS, :].astype(F32).T.astype(BF16)
+        xt[yb, 0] = xe[yb].astype(F32).T.astype(BF16)
         return carry
 
     lax.fori_loop(0, NY, turn, 0)
-    for k in range(1, NZ):
+
+    def x_send(k):
         send(("xz", k), xt.at[t, 0], xt.at[t, k], zdev(-k))
 
-    def a1_take():
+    pair = {"tp": t + 1 - 2 * lax.rem(t, 2)}
+
+    def x_take(j):
+        blk = xt.at[t, j]
+        got(("xz", j), blk)
+        for k in (2, 6):
+            send(("xx", k, j), blk, blk, tdev(k))
+        send(("xc", 0, j), blk, blk, pair)
+
+    def x_mid(j):
+        for k, h in ((2, 0), (6, 128)):
+            row = lax.rem(t + NT - k, NT)
+            blk = xt.at[row, j]
+            got(("xx", k, j), blk)
+            half = xt.at[row, j, pl.ds(h, 128)]
+            send(("xf", k, j), half, half, tdev(k))
+            send(("xc", k, j), blk, blk, pair)
+
+    def x_far(j):
+        row = lax.rem(t + 4, NT)
+        for k, h in ((2, 0), (6, 128)):
+            got(("xf", k, j), xt.at[row, j, pl.ds(h, 128)])
+        blk = xt.at[row, j]
+        send(("xc", 4, j), blk, blk, pair)
+
+    def x_last():
+        for j in range(1, NZ):
+            for k in (0, 2, 6, 4):
+                row = lax.rem(t + 1 - 2 * lax.rem(t, 2) + NT - k, NT)
+                got(("xc", k, j), xt.at[row, j])
+
+    def a1_near():
         for k in (1, -1):
             got(("a1", k), wa.at[y, wrow(zat(-k), 0, 64)])
+            a2_own(1 if k == 1 else 2)
+
+    def a1_far():
         got(("a1", 2), wa.at[y, wrow(zat(2), 0, 32)])
         got(("a1", -2), wa.at[y, wrow(zat(2), 32, 32)])
-        for q in range(NZ):
-            for d in (1, -1):
-                blk = wa.at[y, pl.ds(64 * q, 64)]
-                send(("a2", d, 0, q), blk, blk, ydev(d))
+        a2_own(3)
 
     def a2_last(d):
         return (0, 1) if d == 1 else (2, 3)
@@ -225,7 +303,7 @@
             for d in (1, -1):
                 if s == 4 and q not in a2_last(d):
                     continue
-                blk = wa.at[yat(-d * s), pl.ds(64 * q, 64)]
+                blk = wa.at[yat(-d * s), wrow(zrow(q), 0, 64)]
                 got(("a2", d, s - 1, q), blk)
                 if s < 3 or (s == 3 and q in a2_last(d)):
                     send(("a2", d, s, q), blk, blk, ydev(d))
@@ -263,7 +341,7 @@
             got(("b2f", e, -1), wb.at[yb, wrow(zat(2), 32, 32)])
 
     def project(w, first, width, yb, start):
-        rows = xp[yb]
+        rows = xe[yb]
 
         def tile(c0, n):
             cols = pl.ds(first + c0, n)
@@ -278,6 +356,12 @@
         if width % 256:
             tile(width - width % 256, width % 256)
 
+    def late_project(w, first, c0, n):
+        v = jnp.dot(xl[0], w[0, :, c0 : c0 + n], preferred_element_type=F32)
+        for yb in range(1, NY):
+            v = v + jnp.dot(xl[yb], w[yb, :, c0 : c0 + n], preferred_element_type=F32)
+        prel[:, first + c0 : first + c0 + n] = v
+
     def project_a(s):
         for e in ordinals(s):
             project(wa, 0, CA, yat(-e), s == 0)
@@ -286,101 +370,130 @@
         for e in ordinals(s):
             project(wb, CA, CB, yat(-e), s == 0)
 
+    def turn_cot():
+        for n in range(5):
+            v = cot_ref[n * LANE : (n + 1) * LANE, :].astype(F32).T
+            cot[:, n * LANE : (n + 1) * LANE] = v.astype(BF16)
+        cot[:, 640:768] = jnp.zeros((ROWS, LANE), BF16)
+        cot[:, 640:HALF] = cot_ref[640:HALF, :].astype(F32).T.astype(BF16)
+
+    def tap(cols):
+        return [taps_ref[j : j + 1, cols] for j in range(3)]
+
+    def mixed(src, cols):
+        v = src[:, cols].astype(BF16).astype(F32)
+        w = tap(cols)
+        return v, w[0] * later(v, 2) + w[1] * later(v, 1) + w[2] * v, w
+
+    def back(d, v, w, cols, i, q):
+        r = (w[2] * d + w[1] * sooner(d, 1) + w[0] * sooner(d, 2)).astype(BF16)
+        dpre[:, cols] = r
+        dpq[i, q] = r
+        for j, u in enumerate((later(v, 2), later(v, 1), v)):
+            tsum[q, i, j : j + 1, :] = jnp.sum(d * u, axis=0, keepdims=True) * scale
+
+    def tile_cols(n):
+        return pl.ds(al(n * LANE, LANE), LANE)
+
+    tsum[...] = jnp.zeros_like(tsum)
+    dpq[2, 3] = jnp.zeros((ROWS, LANE), BF16)
+
+    def early_pair(n, gpos, upos, i, q):
+        gc, uc = tile_cols(gpos), tile_cols(upos)
+        gv, gm, gw_ = mixed(pre, gc)
+        uv, um, uw_ = mixed(pre, uc)
+        c = cot[:, tile_cols(n)].astype(F32)
+        act, th = gelu_parts(gm)
+        back(c * um * gelu_slope(gm, th), gv, gw_, gc, i, q)
+        back(c * act, uv, uw_, uc, i, q + 1)
+
+    def early_b(m, carry):
+        early_pair(m + 3, 2 * m + 7, 2 * m + 8, 0, 2 * m)
+        return carry
+
+    def early_a(n, carry):
+        early_pair(n, n, n + 3, 1 + lax.div(n, 2), lax.rem(2 * n, 4))
+        return carry
+
+    last = slice(768, CA)
+
+    def early_last():
+        mv, mm, mw = mixed(pre, last)
+        c = cot[:, 640:768].astype(F32)
+        act, th = gelu_parts(mm)
+        dg = c * swap_halves(mm) * gelu_slope(mm, th)
+        du = swap_halves(c * act)
+        back(jnp.where(low_lanes(dg.shape), dg, du), mv, mw, last, 2, 2)
+
+    def dp_send(i):
+        for k in range(1, NZ):
+            send(("dp", i, k), dpq.at[i, zat(-k)], dpg.at[i, k], zdev(-k))
+        dpg[i, 0] = dpq[i, z]
+
     b1_take(1)
-    a1_take()
+    a1_near()
+    a2_take(1, (0,))
     b2_take(0)
-    order_rows(late_ref, 0)
+    a1_far()
+    x_send(1)
     b1_take(2)
+    x_send(2)
     b2_take(1)
+    a2_take(1, (1,))
+    b1_take(3)
+    x_send(3)
+    pulls[3].wait()
+    order_rows(late_ref, xl)
+    a2_take(1, (2,))
+    b2_take(2)
+    a2_take(1, (3,))
+    x_take(1)
     project_a(0)
-    a2_take(1, (0, 1))
-    b1_take(3)
-    a2_take(1, (2, 3))
-    b2_take(2)
     b1_take(4)
-    for k in range(1, NZ):
-        got(("xz", k), xt.at[t, k])
-    mine = xt.at[t, pl.ds(1, 3)]
-    for k in (2, 4, 6):
-        send(("xx", k), mine, mine, tdev(k))
-    pair = {"tp": t + 1 - 2 * lax.rem(t, 2)}
-    send(("xc", 0), mine, mine, pair)
     project_a(1)
-    a2_take(2, (0, 1))
+    a2_take(2, (0,))
     b2_take(3)
-    a2_take(2, (2, 3))
+    x_take(2)
+    a2_take(2, (1,))
+    x_mid(1)
+    b2_take(4)
+    a2_take(2, (2,))
     b2f_take(0)
+    project_b(0)
+    a2_take(2, (3,))
+    x_take(3)
+    x_mid(2)
+    x_far(1)
+    project_a(2)
     b2f_take(1)
-    b2_take(4)
-    project_a(2)
-    project_b(0)
-    a2_take(3, (0, 1))
-    a2_take(3, (2, 3))
     project_b(1)
-    project_a(3)
+    a2_take(3, (0,))
     b2f_take(2)
     project_b(2)
-    cot[:, 640:CA] = jnp.zeros((ROWS, LANE), BF16)
-    cot[:, 0:HALF] = cot_ref[...]
+    x_mid(3)
+    x_far(2)
+    pulls[4].wait()
+    turn_cot()
+    a2_take(3, (1,))
     b2f_take(3)
     project_b(3)
+    a2_take(3, (2,))
     b2f_take(4)
     project_b(4)
+    lax.fori_loop(0, 2, early_b, 0)
+    dp_send(0)
+    a2_take(3, (3,))
+    x_far(3)
+    project_a(3)
     a2_take(4, range(NZ))
     project_a(4)
-
-    def tap(cols):
-        return [taps_ref[j : j + 1, cols] for j in range(3)]
-
-    def mixed(first, cols):
-        v = pre[first : first + ROWS, cols].astype(BF16).astype(F32)
-        w = tap(cols)
-        return v, w[0] * later(v, 2) + w[1] * later(v, 1) + w[2] * v, w
-
-    def back(d, v, w, cols, n):
-        dpre[:, cols] = (w[2] * d + w[1] * sooner(d, 1) + w[0] * sooner(d, 2)).astype(BF16)
-        q, r = lax.div(n, 3), lax.rem(n, 3)
-        spot = pl.ds(al(r * LANE, LANE), LANE)
-        for j, u in enumerate((later(v, 2), later(v, 1), v)):
-            tsum[q, j : j + 1, spot] = jnp.sum(d * u, axis=0, keepdims=True) * scale
-
-    def tile_cols(n):
-        return pl.ds(al(n * LANE, LANE), LANE)
-
-    tsum[...] = jnp.zeros_like(tsum)
-    dpre[:, WIDE:] = jnp.zeros((ROWS, LANE), BF16)
-
-    def early_tile(n, carry):
-        gc, uc = tile_cols(n), tile_cols(n + 5)
-        gv, gm, gw = mixed(ROWS, gc)
-        uv, um, uw = mixed(ROWS, uc)
-        c = cot[:, gc].astype(F32)
-        act, th = gelu_parts(gm)
-        back(c * um * gelu_slope(gm, th), gv, gw, gc, n)
-        back(c * act, uv, uw, uc, n + 5)
-        return carry
-
-    lax.fori_loop(0, 5, early_tile, 0)
-    last = slice(1280, 1408)
-    mv, mm, mw = mixed(ROWS, last)
-    c = cot[:, 640:CA].astype(F32)
-    act, th = gelu_parts(mm)
-    dg = c * swap_halves(mm) * gelu_slope(mm, th)
-    du = swap_halves(c * act)
-    back(jnp.where(low_lanes(dg.shape), dg, du), mv, mw, last, 10)
-
-    for i in range(3):
-        for k in range(1, NZ):
-            send(
-                ("dp", i, k),
-                dpre.at[:, pl.ds(al((zat(-k) * 3 + i) * LANE, LANE), LANE)],
-                dpg.at[i, k],
-                zdev(-k),
-            )
+    lax.fori_loop(0, 2, early_a, 0)
+    dp_send(1)
+    lax.fori_loop(2, 3, early_a, 0)
+    early_last()
     for k in range(1, NZ):
         send(("tz", k), tsum.at[zat(-k)], tzr.at[k], zdev(-k))
-    for i in range(3):
-        dpg[i, 0] = dpre[:, pl.ds(al((z * 3 + i) * LANE, LANE), LANE)]
+    dp_send(2)
 
     def dx(yb, carry):
         nt = (((1,), (1,)), ((), ()))
@@ -389,30 +502,20 @@
         dxp[:, pl.ds(al(yb * 256, 256), 256)] = v.astype(BF16)
         return carry
 
-    lax.fori_loop(0, NY, dx, 0)
-
     def strip(tt):
         return pl.ds(al(tt * 32, 32), 32)
 
-    for k in range(1, NT):
-        to = lax.rem(t + NT - k, NT)
-        send(("dx", k), dxp.at[strip(to)], dxr.at[k], tdev(-k))
-
-    for k in (2, 4, 6):
-        row = lax.rem(t + NT - k, NT)
-        blk = xt.at[row, pl.ds(1, 3)]
-        got(("xx", k), blk)
-        send(("xc", k), blk, blk, pair)
-
-    for k in range(1, NZ):
-        got(("tz", k), tzr.at[k])
-    tys[...] = tsum[z] + tzr[1] + tzr[2] + tzr[3]
-    for k in range(1, NY):
-        send(("ty", k), tys, tyr.at[k], ydev(-k))
-
-    for k in (0, 2, 4, 6):
-        row = lax.rem(t + 1 - 2 * lax.rem(t, 2) + NT - k, NT)
-        got(("xc", k), xt.at[row, pl.ds(1, 3)])
+    def dx_send():
+        for k in range(1, NT):
+            to = lax.rem(t + NT - k, NT)
+            send(("dx", k), dxp.at[strip(to)], dxr.at[k], tdev(-k))
+
+    def taps_first():
+        for k in range(1, NZ):
+            got(("tz", k), tzr.at[k])
+        tys[...] = tsum[z] + tzr[1] + tzr[2] + tzr[3]
+        for k in range(1, NY):
+            send(("ty", k), tys, tyr.at[k], ydev(-k))
 
     def term(i, yb):
         v = jnp.dot(xt[yb, 0], dpg[i, 0], preferred_element_type=F32)
@@ -490,57 +593,75 @@
         for k in range(1, NZ):
             send(("tf", k), tfr.at[0], tfr.at[k], zdev(-k))
 
-    def late_tile(n, carry):
-        gc = tile_cols(n)
-        _, gm, _ = mixed(0, gc)
-        _, um, _ = mixed(0, tile_cols(n + 5))
+    def late_pair(n, gpos, upos):
+        _, gm, _ = mixed(prel, tile_cols(gpos))
+        _, um, _ = mixed(prel, tile_cols(upos))
         act, _ = gelu_parts(gm)
-        hid_ref[:, gc] = (act * um).astype(BF16)
+        hid_ref[tile_cols(n), :] = (act * um).T.astype(BF16)
+
+    def late_b(m, carry):
+        late_pair(m + 3, 2 * m + 7, 2 * m + 8)
         return carry
 
+    def late_a(n, carry):
+        late_pair(n, n, n + 3)
+        return carry
+
+    def late_last():
+        _, mm, _ = mixed(prel, last)
+        act, _ = gelu_parts(mm)
+        hid_ref[640:HALF, :] = (act * swap_halves(mm)).T[0:64].astype(BF16)
+
+    x_last()
     rs(0, 0)
-    lax.fori_loop(0, 5, late_tile, 0)
-    _, mm, _ = mixed(0, last)
-    act, _ = gelu_parts(mm)
-    hid_ref[:, 640:HALF] = (act * swap_halves(mm)).astype(BF16)[:, 0:64]
+    lax.fori_loop(0, NY, dx, 0)
+    dx_send()
     rs(0, 1)
+    late_project(wa, 0, 0, 256)
+    late_project(wa, 0, 256, 256)
+    rs(0, 2)
     rs(1, 0)
-    rs(0, 2)
+    late_project(wa, 0, 512, 256)
     rs(1, 1)
+    rs(0, 3)
     dx_reduce()
-    rs(0, 3)
+    late_project(wa, 0, 768, 128)
     rs(2, 0)
     rs(1, 2)
-    taps_finish()
+    taps_first()
+    rs(0, 4)
+    late_project(wb, CA, 0, 256)
     rs(2, 1)
-    rs(0, 4)
     rs(1, 3)
+    late_project(wb, CA, 256, 256)
     rs(2, 2)
     rs(1, 4)
+    lax.fori_loop(0, 3, late_a, 0)
     rs(2, 3)
+    taps_finish()
+    lax.fori_loop(0, 2, late_b, 0)
+    late_last()
     rs(2, 4)
 
-    def tile_out(n, v):
-        if n < 5:
-            cols = slice(n * LANE, (n + 1) * LANE)
-            gnext_ref[:, cols] = gsum_ref[:, cols] + v
-        elif n < 10:
-            cols = slice((n - 5) * LANE, (n - 4) * LANE)
-            unext_ref[:, cols] = usum_ref[:, cols] + v
-        else:
-            gnext_ref[:, 640:HALF] = gsum_ref[:, 640:HALF] + v[:, 0:64]
-            unext_ref[:, 640:HALF] = usum_ref[:, 640:HALF] + swap_halves(v)[:, 0:64]
-
-    def taps_out(n, v):
-        if n < 5:
-            cols = slice(n * LANE, (n + 1) * LANE)
-            gtnext_ref[:, cols] = gtsum_ref[:, cols] + v[0:3]
-        elif n < 10:
-            cols = slice((n - 5) * LANE, (n - 4) * LANE)
-            utnext_ref[:, cols] = utsum_ref[:, cols] + v[0:3]
-        else:
+    def spread(pos, v, prev, nxt):
+        (gs, us), (gn, un) = prev, nxt
+        if pos == 6:
+            gn[:, 640:HALF] = gs[:, 640:HALF] + v[:, 0:64]
+            un[:, 640:HALF] = us[:, 640:HALF] + swap_halves(v)[:, 0:64]
+            return
+        side_, n = (0, GPOS.index(pos)) if pos in GPOS else (1, UPOS.index(pos))
+        cols = slice(n * LANE, (n + 1) * LANE)
+        nxt[side_][:, cols] = prev[side_][:, cols] + v
+
+    def tile_out(pos, v):
+        spread(pos, v, (gsum_ref, usum_ref), (gnext_ref, unext_ref))
+
+    def taps_out(pos, v):
+        if pos == 6:
             gtnext_ref[:, 640:HALF] = gtsum_ref[:, 640:HALF] + v[0:3, 0:64]
             utnext_ref[:, 640:HALF] = utsum_ref[:, 640:HALF] + swap_halves(v)[0:3, 0:64]
+            return
+        spread(pos, v[0:3], (gtsum_ref, utsum_ref), (gtnext_ref, utnext_ref))
 
     for k in range(1, NZ):
         got(("tf", k), tfr.at[k])
@@ -549,11 +670,13 @@
     for i in range(3):
         for k in range(1, NZ):
             got(("fin", i, k), finr.at[k, i])
-    for n in range(11):
-        k = lax.rem(n // 3 + NZ - z, NZ)
-        tile_out(n, finr[k, n % 3].astype(F32))
-        v = tfr[k]
-        taps_out(n, v[:, (n % 3) * LANE : (n % 3 + 1) * LANE])
+    pulls[5].wait()
+    pulls[6].wait()
+    for i, tiles in enumerate(((7, 8, 9, 10), (0, 3, 1, 4), (2, 5, 6))):
+        for q, n in enumerate(tiles):
+            k = lax.rem(q + NZ - z, NZ)
+            tile_out(n, finr[k, i].astype(F32))
+            taps_out(n, tfr[k, i])
     for c in sent:
         c.wait_send()
 
@@ -571,34 +694,42 @@
     gate_taps_sum,
     up_taps_sum,
 ):
-    def joined(g, u):
-        return jnp.concatenate([g[:, :640], u[:, :640], g[:, 640:], u[:, 640:]], axis=1)
-
-    weight = joined(gate_weight, up_weight)
-    taps = joined(gate_taps, up_taps).astype(F32)
     vmem = pl.BlockSpec(memory_space=pltpu.VMEM)
     shapes = (
-        ((ROWS, HALF), BF16),
+        ((HALF, ROWS), BF16),
         ((ROWS, 2048), BF16),
         ((64, HALF), F32),
         ((64, HALF), F32),
         ((3, HALF), F32),
         ((3, HALF), F32),
     )
-    n_sem = 170
-    return pl.pallas_call(
+    n_sem = 190
+    hbm = pl.BlockSpec(memory_space=pltpu.HBM)
+    hid, *rest = pl.pallas_call(
         kernel,
-        out_shape=[jax.ShapeDtypeStruct(s, d) for s, d in shapes],
-        in_specs=[vmem] * 9,
+        out_shape=[pltpu.VMEM(s, d) for s, d in shapes],
+        in_specs=[hbm] * 7 + [vmem] * 4,
         out_specs=[vmem] * 6,
         scratch_shapes=[
+            pltpu.VMEM((ROWS, 2048), BF16),
+            pltpu.VMEM((ROWS, 2048), BF16),
+            pltpu.VMEM((HALF, ROWS), BF16),
+            pltpu.VMEM((64, HALF), BF16),
+            pltpu.VMEM((64, HALF), BF16),
+            pltpu.VMEM((64, HALF), F32),
+            pltpu.VMEM((64, HALF), F32),
+            pltpu.VMEM((64, LANE), F32),
+            pltpu.VMEM((8, WIDE), F32),
             pltpu.VMEM((NY, 256, CA), BF16),
             pltpu.VMEM((NY, 256, CB), BF16),
-            pltpu.VMEM((NY, 2 * ROWS, 256), BF16),
+            pltpu.VMEM((NY, ROWS, 256), BF16),
+            pltpu.VMEM((NY, ROWS, 256), BF16),
             pltpu.VMEM((NY, NZ, 256, ROWS), BF16),
-            pltpu.VMEM((2 * ROWS, WIDE), F32),
-            pltpu.VMEM((ROWS, CA), BF16),
-            pltpu.VMEM((ROWS, WIDE + LANE), BF16),
+            pltpu.VMEM((ROWS, WIDE), F32),
+            pltpu.VMEM((ROWS, WIDE), F32),
+            pltpu.VMEM((ROWS, 768), BF16),
+            pltpu.VMEM((ROWS, WIDE), BF16),
+            pltpu.VMEM((3, NZ, ROWS, LANE), BF16),
             pltpu.VMEM((3, NZ, ROWS, LANE), BF16),
             pltpu.VMEM((2, 3, 4, 256, LANE), BF16),
             pltpu.VMEM((2, 3, 4, 256, LANE), BF16),
@@ -607,28 +738,32 @@
             pltpu.VMEM((ROWS, 2048), BF16),
             pltpu.VMEM((NT, 32, 2048), BF16),
             pltpu.VMEM((32, 2048), BF16),
-            pltpu.VMEM((NZ, 8, 384), F32),
-            pltpu.VMEM((NZ, 8, 384), F32),
-            pltpu.VMEM((8, 384), F32),
-            pltpu.VMEM((NY, 8, 384), F32),
-            pltpu.VMEM((NZ, 8, 384), F32),
+            pltpu.VMEM((NZ, 3, 8, LANE), F32),
+            pltpu.VMEM((NZ, 3, 8, LANE), F32),
+            pltpu.VMEM((3, 8, LANE), F32),
+            pltpu.VMEM((NY, 3, 8, LANE), F32),
+            pltpu.VMEM((NZ, 3, 8, LANE), F32),
+            pltpu.SemaphoreType.DMA((7,)),
             pltpu.SemaphoreType.DMA((n_sem,)),
             pltpu.SemaphoreType.DMA((n_sem,)),
         ],
         compiler_params=pltpu.CompilerParams(
-            collective_id=0, has_side_effects=True, vmem_limit_bytes=60 * 1024 * 1024
+            collective_id=0, has_side_effects=True, vmem_limit_bytes=57000 * 1024
         ),
     )(
         late_rows,
         early_rows,
-        hidden_cot,
-        weight,
-        taps,
+        hidden_cot.T,
+        gate_weight,
+        up_weight,
         gate_grad_sum,
         up_grad_sum,
+        gate_taps,
+        up_taps,
         gate_taps_sum,
         up_taps_sum,
     )
+    return (hid.T, *rest)
 
 
 def solution(mesh):

time: 131 us -> 108 us (0.82)
  Pallas kernels: 117 us -> 102 us
  local copies, waits for them, and re-layouts: 10.7 us -> 4.26 us
    pallas_call x1, Pallas kernels: 117 us -> 102 us  [per_device(): pl.pallas_call(kernel, out_shape=[pltpu.VMEM(s, d) for s, d in shapes], i...]
    unnamed x16 -> x6, local copies, waits for them, and re-layouts: 6.28 us -> 4.26 us
    pallas_call x1 -> x0, local copies, waits for them, and re-layouts: 1.9 us -> none  [per_device(): pl.pallas_call(kernel, out_shape=[jax.ShapeDtypeStruct(s, d) for s, d in...]
    slice x16 -> x0, local copies, waits for them, and re-layouts: 1.64 us -> none  [the longest x4 0.71 us: joined(): u[:, :640]]
where the time goes in v2:
time: 108 us; the launch traced here: 107 us
  Pallas kernels  102 us (94%)
  local copies, waits for them, and re-layouts  4.26 us (4%)
    pallas_call x1, Pallas kernels, per_device(): pl.pallas_call(kernel, out_shape=[pltpu.VMEM(s, d) for s, d in shapes], i...  102 us
    unnamed x6, local copies, waits for them, and re-layouts  4.26 us

profile of v2, /device:TPU:6, one launch (start us, length us, event | category | flops | bytes accessed | tf_op | source)
XLA Modules:
  0.0 107.1 jit_solution(4934127335291448757)
XLA Ops:
  0.6 102.2 %shard_map.154 = (bf16[704,256]{1,0:T(8,128)(2,1)S(1)}, bf16[256,2048]{1,0:T(8,128)(2,1)S(1)}, f32[64,704]{1,0:T(8,128)S(1)}, f32[64,704]{1,0:T(8,128)S(1)}, f32[3,704]{1,0:T(4,128)S(1)}, /*index=5*/f32[3,704]{1,0:T(4,128)S(1)}) custom-call(bf16[256,2048]{1,0:T(8,128)(2,1)} %late_hbm.1, bf16[256,2048]{1,0:T(8,128)(2,1)} %early_hbm.1, ...), custom_call_target="tpu_custom_call" | custom-call | tf_op jit(solution)/shard_map/pallas_call | solution.py:708
  102.8 0.7 copy.23
  103.6 0.6 copy.27
  104.2 0.6 copy.28
  104.8 0.7 copy.25
  105.4 0.7 copy.26
  106.1 1.0 copy.24

commit v3 on v2

--- a/solution.py
+++ b/solution.py
@@ -13,10 +13,11 @@
 NZ, NY, NT = 4, 8, 8
 ROWS = 256
 LANE = 128
-CA, CB = 896, 512
-WIDE = CA + CB
+CA, CC, CB = 512, 384, 512
+AC = CA + CC
+WIDE = AC + CB
 HALF = 704
-GPOS, UPOS = (0, 1, 2, 7, 9), (3, 4, 5, 8, 10)
+GPOS, UPOS = (0, 2, 4, 7, 9), (1, 3, 5, 8, 10)
 F32, BF16 = jnp.float32, jnp.bfloat16
 GELU_K = 0.7978845608028654
 GELU_A = 0.044715
@@ -64,10 +65,10 @@
     uw_hbm,
     gsum_hbm,
     usum_hbm,
-    gt_ref,
-    ut_ref,
-    gtsum_ref,
-    utsum_ref,
+    gt_hbm,
+    ut_hbm,
+    gtsum_hbm,
+    utsum_hbm,
     hid_ref,
     eg_ref,
     gnext_ref,
@@ -81,9 +82,14 @@
     uw,
     gsum_ref,
     usum_ref,
+    gt_ref,
+    ut_ref,
+    gtsum_ref,
+    utsum_ref,
     wmix,
     taps_ref,
     wa,
+    wc,
     wb,
     xe,
     xl,
@@ -99,6 +105,8 @@
     fin,
     finr,
     dxp,
+    dxc,
+    dxs,
     dxr,
     egs,
     tsum,
@@ -154,6 +162,10 @@
             (cot_hbm, cot_ref),
             (gsum_hbm, gsum_ref),
             (usum_hbm, usum_ref),
+            (gt_hbm, gt_ref),
+            (ut_hbm, ut_ref),
+            (gtsum_hbm, gtsum_ref),
+            (utsum_hbm, utsum_ref),
         )
     ):
         c = pltpu.make_async_copy(src, dst, lsem.at[n])
@@ -194,16 +206,15 @@
     pulls[1].wait()
     wmix[:, 0:64] = gw[:, 640:HALF].astype(F32)
     wmix[:, 64:LANE] = uw[:, 640:HALF].astype(F32)
-    taps_ref[0:3, 768:832] = gt_ref[:, 640:HALF].astype(F32)
-    taps_ref[0:3, 832:CA] = ut_ref[:, 640:HALF].astype(F32)
-    wa[y, own, 768:CA] = wmix[...].astype(BF16)
+    wc[y, own, 256:CC] = wmix[...].astype(BF16)
     for n in range(5):
         cols = slice(n * LANE, (n + 1) * LANE)
-        for src, tsrc, pos in ((gw, gt_ref, GPOS[n]), (uw, ut_ref, UPOS[n])):
+        for src, pos in ((gw, GPOS[n]), (uw, UPOS[n])):
             here = slice(pos * LANE, (pos + 1) * LANE)
-            taps_ref[0:3, here] = tsrc[:, cols].astype(F32)
-            if pos < 7:
+            if pos < 4:
                 wa[y, own, here] = src[:, cols]
+            elif pos < 7:
+                wc[y, own, (pos - 4) * LANE : (pos - 3) * LANE] = src[:, cols]
             else:
                 wb[y, own, (pos - 7) * LANE : (pos - 6) * LANE] = src[:, cols]
     pl.semaphore_wait(barrier, len(peers))
@@ -211,23 +222,34 @@
     def zrow(q):
         return zat((0, -1, 1, 2)[q])
 
-    def a2_own(q):
-        blk = wa.at[y, wrow(zrow(q), 0, 64)]
+    wide = {"a": wa, "c": wc}
+
+    def a2_own(p, q):
+        blk = wide[p].at[y, wrow(zrow(q), 0, 64)]
         for d in (1, -1):
-            send(("a2", d, 0, q), blk, blk, ydev(d))
-
-    a_own, b_own = wa.at[y, own], wb.at[y, own]
-    for k in (1, -1):
-        send(("a1", k), a_own, a_own, ring(k))
+            send(("a2", p, d, 0, q), blk, blk, ydev(d))
+
+    def a1_send(p, near):
+        if near:
+            blk = wide[p].at[y, own]
+            for k in (1, -1):
+                send(("a1", p, k), blk, blk, ring(k))
+            return
+        for h, k in ((0, 2), (1, -2)):
+            blk = wide[p].at[y, wrow(z, 32 * h, 32)]
+            send(("a1", p, k), blk, blk, ring(k))
+
+    b_own = wb.at[y, own]
+    a1_send("a", True)
     for h, d in ((0, 1), (1, -1), (1, 1), (0, -1)):
         blk = wb.at[y, wrow(z, 32 * h, 32)]
         send(("b1", d, 0, h), blk, blk, ydev(d))
-    for h, k in ((0, 2), (1, -2)):
-        blk = wa.at[y, wrow(z, 32 * h, 32)]
-        send(("a1", k), blk, blk, ring(k))
-    a2_own(0)
+    a1_send("a", False)
+    a2_own("a", 0)
     for k in (1, -1):
         send(("b2", 0, k), b_own, b_own, ring(k))
+    a1_send("c", True)
+    a1_send("c", False)
 
     def order_rows(src_ref, dst):
         def one(yp, carry):
@@ -285,28 +307,26 @@
                 row = lax.rem(t + 1 - 2 * lax.rem(t, 2) + NT - k, NT)
                 got(("xc", k, j), xt.at[row, j])
 
-    def a1_near():
+    def a1_near(p):
         for k in (1, -1):
-            got(("a1", k), wa.at[y, wrow(zat(-k), 0, 64)])
-            a2_own(1 if k == 1 else 2)
-
-    def a1_far():
-        got(("a1", 2), wa.at[y, wrow(zat(2), 0, 32)])
-        got(("a1", -2), wa.at[y, wrow(zat(2), 32, 32)])
-        a2_own(3)
+            got(("a1", p, k), wide[p].at[y, wrow(zat(-k), 0, 64)])
+
+    def a1_far(p):
+        got(("a1", p, 2), wide[p].at[y, wrow(zat(2), 0, 32)])
+        got(("a1", p, -2), wide[p].at[y, wrow(zat(2), 32, 32)])
 
     def a2_last(d):
         return (0, 1) if d == 1 else (2, 3)
 
-    def a2_take(s, qs):
+    def a2_take(p, s, qs):
         for q in qs:
             for d in (1, -1):
                 if s == 4 and q not in a2_last(d):
                     continue
-                blk = wa.at[yat(-d * s), wrow(zrow(q), 0, 64)]
-                got(("a2", d, s - 1, q), blk)
+                blk = wide[p].at[yat(-d * s), wrow(zrow(q), 0, 64)]
+                got(("a2", p, d, s - 1, q), blk)
                 if s < 3 or (s == 3 and q in a2_last(d)):
-                    send(("a2", d, s, q), blk, blk, ydev(d))
+                    send(("a2", p, d, s, q), blk, blk, ydev(d))
 
     def b1_take(s):
         for d in (1, -1):
@@ -366,9 +386,23 @@
         for e in ordinals(s):
             project(wa, 0, CA, yat(-e), s == 0)
 
+    def project_c(s):
+        for e in ordinals(s):
+            project(wc, CA, CC, yat(-e), s == 0)
+
     def project_b(s):
         for e in ordinals(s):
-            project(wb, CA, CB, yat(-e), s == 0)
+            project(wb, AC, CB, yat(-e), s == 0)
+
+    def join_taps():
+        for n in range(7, 11):
+            pulls[n].wait()
+        for n in range(5):
+            cols = slice(n * LANE, (n + 1) * LANE)
+            for src, pos in ((gt_ref, GPOS[n]), (ut_ref, UPOS[n])):
+                taps_ref[0:3, pos * LANE : (pos + 1) * LANE] = src[:, cols].astype(F32)
+        taps_ref[0:3, 768:832] = gt_ref[:, 640:HALF].astype(F32)
+        taps_ref[0:3, 832:AC] = ut_ref[:, 640:HALF].astype(F32)
 
     def turn_cot():
         for n in range(5):
@@ -407,108 +441,57 @@
         back(c * um * gelu_slope(gm, th), gv, gw_, gc, i, q)
         back(c * act, uv, uw_, uc, i, q + 1)
 
+    def early_a(n, carry):
+        early_pair(n, 2 * n, 2 * n + 1, 0, 2 * n)
+        return carry
+
     def early_b(m, carry):
-        early_pair(m + 3, 2 * m + 7, 2 * m + 8, 0, 2 * m)
+        early_pair(m + 3, 2 * m + 7, 2 * m + 8, 1, 2 * m)
         return carry
 
-    def early_a(n, carry):
-        early_pair(n, n, n + 3, 1 + lax.div(n, 2), lax.rem(2 * n, 4))
-        return carry
-
-    last = slice(768, CA)
-
-    def early_last():
+    last = slice(768, AC)
+
+    def early_c():
+        early_pair(2, 4, 5, 2, 0)
         mv, mm, mw = mixed(pre, last)
         c = cot[:, 640:768].astype(F32)
         act, th = gelu_parts(mm)
         dg = c * swap_halves(mm) * gelu_slope(mm, th)
         du = swap_halves(c * act)
         back(jnp.where(low_lanes(dg.shape), dg, du), mv, mw, last, 2, 2)
+        for k in range(1, NZ):
+            send(("tz", k), tsum.at[zat(-k)], tzr.at[k], zdev(-k))
 
     def dp_send(i):
         for k in range(1, NZ):
             send(("dp", i, k), dpq.at[i, zat(-k)], dpg.at[i, k], zdev(-k))
         dpg[i, 0] = dpq[i, z]
 
-    b1_take(1)
-    a1_near()
-    a2_take(1, (0,))
-    b2_take(0)
-    a1_far()
-    x_send(1)
-    b1_take(2)
-    x_send(2)
-    b2_take(1)
-    a2_take(1, (1,))
-    b1_take(3)
-    x_send(3)
-    pulls[3].wait()
-    order_rows(late_ref, xl)
-    a2_take(1, (2,))
-    b2_take(2)
-    a2_take(1, (3,))
-    x_take(1)
-    project_a(0)
-    b1_take(4)
-    project_a(1)
-    a2_take(2, (0,))
-    b2_take(3)
-    x_take(2)
-    a2_take(2, (1,))
-    x_mid(1)
-    b2_take(4)
-    a2_take(2, (2,))
-    b2f_take(0)
-    project_b(0)
-    a2_take(2, (3,))
-    x_take(3)
-    x_mid(2)
-    x_far(1)
-    project_a(2)
-    b2f_take(1)
-    project_b(1)
-    a2_take(3, (0,))
-    b2f_take(2)
-    project_b(2)
-    x_mid(3)
-    x_far(2)
-    pulls[4].wait()
-    turn_cot()
-    a2_take(3, (1,))
-    b2f_take(3)
-    project_b(3)
-    a2_take(3, (2,))
-    b2f_take(4)
-    project_b(4)
-    lax.fori_loop(0, 2, early_b, 0)
-    dp_send(0)
-    a2_take(3, (3,))
-    x_far(3)
-    project_a(3)
-    a2_take(4, range(NZ))
-    project_a(4)
-    lax.fori_loop(0, 2, early_a, 0)
-    dp_send(1)
-    lax.fori_loop(2, 3, early_a, 0)
-    early_last()
-    for k in range(1, NZ):
-        send(("tz", k), tsum.at[zat(-k)], tzr.at[k], zdev(-k))
-    dp_send(2)
-
     def dx(yb, carry):
         nt = (((1,), (1,)), ((), ()))
         v = lax.dot_general(dpre[:, 0:CA], wa[yb], nt, preferred_element_type=F32)
-        v = v + lax.dot_general(dpre[:, CA:WIDE], wb[yb], nt, preferred_element_type=F32)
+        v = v + lax.dot_general(dpre[:, CA:AC], wc[yb], nt, preferred_element_type=F32)
+        v = v + lax.dot_general(dpre[:, AC:WIDE], wb[yb], nt, preferred_element_type=F32)
         dxp[:, pl.ds(al(yb * 256, 256), 256)] = v.astype(BF16)
         return carry
 
     def strip(tt):
         return pl.ds(al(tt * 32, 32), 32)
 
+    core = lax.rem(t, 2)
+
     def dx_send():
-        for k in range(1, NT):
-            to = lax.rem(t + NT - k, NT)
-            send(("dx", k), dxp.at[strip(to)], dxr.at[k], tdev(-k))
+        for x in range(4):
+            send(("dc", x), dxp.at[strip(2 * x + 1 - core)], dxc.at[x], pair)
+
+    def dx_pair():
+        for x in range(4):
+            got(("dc", x), dxc.at[x])
+            v = dxp[strip(2 * x + core), :].astype(F32) + dxc[x].astype(F32)
+            dxs[x] = v.astype(BF16)
+        for k in (2, 6, 4):
+            to = lax.div(lax.rem(t + NT - k, NT), 2)
+            send(("dx", k), dxs.at[to], dxr.at[k // 2], tdev(-k))
 
     def taps_first():
         for k in range(1, NZ):
@@ -533,45 +516,50 @@
         if s == 0:
             for k in range(1, NZ):
                 got(("dp", i, k), dpg.at[i, k])
+            for d in (1, -1):
+                buf = snd.at[side(d), i, 0]
+                buf[...] = term(i, yat(3 * d)).astype(BF16)
+                send(("rs", i, 0, d), buf, rcv.at[side(d), i, 0], ydev(d))
             v = term(i, yat(4))
             for d in (1, -1):
-                buf = snd.at[side(d), i, 0, part(d)]
+                buf = snd.at[side(d), i, 3, part(d)]
                 buf[...] = (v[0:128] if d == 1 else v[128:256]).astype(BF16)
-                send(("rs", i, 0, d), buf, rcv.at[side(d), i, 0, part(d)], ydev(d))
+                send(("rs", i, 3, d), buf, rcv.at[side(d), i, 3, part(d)], ydev(2 * d))
             return
-        if s < 4:
+        if s < 3:
             for d in (1, -1):
-                snd_f = term(i, yat(d * (4 - s)))
+                v = term(i, yat(d * (3 - s)))
+                got(("rs", i, s - 1, d), rcv.at[side(d), i, s - 1])
+                v = v + rcv[side(d), i, s - 1].astype(F32)
                 buf = snd.at[side(d), i, s]
                 if s == 1:
-                    got(("rs", i, 0, d), rcv.at[side(d), i, 0, part(d)])
-                    in_ = rcv[side(d), i, 0, part(d), :].astype(F32)
+                    far = rcv.at[side(d), i, 3, part(d)]
+                    got(("rs", i, 3, d), far)
+                    w = far[...].astype(F32)
                     if d == 1:
-                        buf[0:128, :] = (snd_f[0:128] + in_).astype(BF16)
-                        buf[128:256, :] = snd_f[128:256].astype(BF16)
+                        buf[0:128, :] = (v[0:128] + w).astype(BF16)
+                        buf[128:256, :] = v[128:256].astype(BF16)
                     else:
-                        buf[0:128, :] = snd_f[0:128].astype(BF16)
-                        buf[128:256, :] = (snd_f[128:256] + in_).astype(BF16)
+                        buf[0:128, :] = v[0:128].astype(BF16)
+                        buf[128:256, :] = (v[128:256] + w).astype(BF16)
                 else:
-                    got(("rs", i, s - 1, d), rcv.at[side(d), i, s - 1])
-                    buf[...] = (snd_f + rcv[side(d), i, s - 1].astype(F32)).astype(BF16)
+                    buf[...] = v.astype(BF16)
                 send(("rs", i, s, d), buf, rcv.at[side(d), i, s], ydev(d))
             return
         v = term(i, y)
         for d in (1, -1):
-            got(("rs", i, 3, d), rcv.at[side(d), i, 3])
-            v = v + rcv[side(d), i, 3].astype(F32)
+            got(("rs", i, 2, d), rcv.at[side(d), i, 2])
+            v = v + rcv[side(d), i, 2].astype(F32)
         fin[i] = v.astype(BF16)
         for k in range(1, NZ):
             send(("fin", i, k), fin.at[i, wrow(zat(-k), 0, 64)], finr.at[k, i], zdev(-k))
         finr[0, i] = fin[i, own, :]
 
     def dx_reduce():
-        for k in range(1, NT):
-            got(("dx", k), dxr.at[k])
-        v = dxp[strip(t), :].astype(F32)
-        for k in range(1, NT):
-            v = v + dxr[k].astype(F32)
+        v = dxs[lax.div(t, 2)].astype(F32)
+        for k in (2, 6, 4):
+            got(("dx", k), dxr.at[k // 2])
+            v = v + dxr[k // 2].astype(F32)
         for yp in range(NY // 2):
             for zp in range(2):
                 a = v[:, 2 * yp * 256 + zp * LANE : 2 * yp * 256 + (zp + 1) * LANE]
@@ -580,9 +568,21 @@
                 at0 = 2 * zp * 512 + yp * LANE
                 egs[:, at0 : at0 + LANE] = jnp.where(low, a, swap_halves(b)).astype(BF16)
                 egs[:, at0 + 512 : at0 + 512 + LANE] = jnp.where(low, swap_halves(a), b).astype(BF16)
-        for k in range(1, NT):
-            send(("eg", k), egs, eg_ref.at[strip(t)], tdev(-k))
+        for k in (2, 6, 4):
+            send(("eg", k), egs, eg_ref.at[strip(t)], tdev(k))
+        send(("ec", 0), egs, eg_ref.at[strip(t)], pair)
         eg_ref[strip(t), :] = egs[...]
+
+    def eg_cross():
+        for k in (2, 6, 4):
+            here = eg_ref.at[strip(lax.rem(t + NT - k, NT))]
+            got(("eg", k), here)
+            send(("ec", k), here, here, pair)
+
+    def eg_last():
+        for k in (0, 2, 6, 4):
+            row = lax.rem(t + 1 - 2 * lax.rem(t, 2) + NT - k, NT)
+            got(("ec", k), eg_ref.at[strip(row)])
 
     def taps_finish():
         v = tys[...]
@@ -599,49 +599,134 @@
         act, _ = gelu_parts(gm)
         hid_ref[tile_cols(n), :] = (act * um).T.astype(BF16)
 
+    def late_a(n, carry):
+        late_pair(n, 2 * n, 2 * n + 1)
+        return carry
+
     def late_b(m, carry):
         late_pair(m + 3, 2 * m + 7, 2 * m + 8)
         return carry
 
-    def late_a(n, carry):
-        late_pair(n, n, n + 3)
-        return carry
-
-    def late_last():
+    def late_c():
+        late_pair(2, 4, 5)
         _, mm, _ = mixed(prel, last)
         act, _ = gelu_parts(mm)
         hid_ref[640:HALF, :] = (act * swap_halves(mm)).T[0:64].astype(BF16)
 
+    b1_take(1)
+    a1_near("a")
+    a2_own("a", 1)
+    a2_own("a", 2)
+    a2_take("a", 1, (0,))
+    a1_far("a")
+    a2_own("a", 3)
+    b2_take(0)
+    x_send(1)
+    a2_take("a", 1, (1,))
+    b1_take(2)
+    x_send(2)
+    a2_take("a", 1, (2,))
+    a2_take("a", 1, (3,))
+    b2_take(1)
+    x_send(3)
+    pulls[3].wait()
+    order_rows(late_ref, xl)
+    b1_take(3)
+    a2_take("a", 2, (0, 1))
+    project_a(0)
+    a2_take("a", 2, (2, 3))
+    b2_take(2)
+    b1_take(4)
+    x_take(1)
+    a1_near("c")
+    a1_far("c")
+    a2_take("a", 3, (0,))
+    a2_own("c", 0)
+    project_a(1)
+    a2_take("a", 3, (1,))
+    a2_own("c", 1)
+    a2_take("a", 3, (2,))
+    a2_own("c", 2)
+    a2_take("a", 3, (3,))
+    a2_own("c", 3)
+    x_take(2)
+    project_a(2)
+    a2_take("a", 4, range(NZ))
+    a2_take("c", 1, (0,))
+    b2_take(3)
+    project_a(3)
+    a2_take("c", 1, (1,))
+    x_mid(1)
+    pulls[4].wait()
+    turn_cot()
+    join_taps()
+    a2_take("c", 1, (2,))
+    project_a(4)
+    lax.fori_loop(0, 2, early_a, 0)
+    dp_send(0)
+    a2_take("c", 1, (3,))
+    b2_take(4)
+    x_take(3)
+    a2_take("c", 2, (0,))
+    x_mid(2)
+    x_far(1)
+    a2_take("c", 2, (1,))
+    b2f_take(0)
+    project_b(0)
+    b2f_take(1)
+    project_b(1)
+    a2_take("c", 2, (2, 3))
+    b2f_take(2)
+    project_b(2)
+    a2_take("c", 3, (0,))
+    x_mid(3)
+    x_far(2)
+    project_c(0)
+    a2_take("c", 3, (1,))
+    b2f_take(3)
+    project_b(3)
+    a2_take("c", 3, (2, 3))
+    b2f_take(4)
+    project_b(4)
+    lax.fori_loop(0, 2, early_b, 0)
+    dp_send(1)
+    project_c(1)
+    project_c(2)
+    project_c(3)
+    x_far(3)
+    a2_take("c", 4, range(NZ))
+    project_c(4)
+    early_c()
+    dp_send(2)
     x_last()
     rs(0, 0)
     lax.fori_loop(0, NY, dx, 0)
     dx_send()
     rs(0, 1)
+    rs(1, 0)
+    dx_pair()
+    taps_first()
     late_project(wa, 0, 0, 256)
+    rs(0, 2)
+    rs(1, 1)
+    rs(2, 0)
     late_project(wa, 0, 256, 256)
-    rs(0, 2)
-    rs(1, 0)
-    late_project(wa, 0, 512, 256)
-    rs(1, 1)
     rs(0, 3)
+    rs(1, 2)
+    rs(2, 1)
     dx_reduce()
-    late_project(wa, 0, 768, 128)
-    rs(2, 0)
-    rs(1, 2)
-    taps_first()
-    rs(0, 4)
-    late_project(wb, CA, 0, 256)
-    rs(2, 1)
+    late_project(wc, CA, 0, 256)
+    late_project(wc, CA, 256, 128)
     rs(1, 3)
-    late_project(wb, CA, 256, 256)
     rs(2, 2)
-    rs(1, 4)
-    lax.fori_loop(0, 3, late_a, 0)
+    late_project(wb, AC, 0, 256)
+    late_project(wb, AC, 256, 256)
+    taps_finish()
+    eg_cross()
+    lax.fori_loop(0, 2, late_a, 0)
     rs(2, 3)
-    taps_finish()
     lax.fori_loop(0, 2, late_b, 0)
-    late_last()
-    rs(2, 4)
+    late_c()
 
     def spread(pos, v, prev, nxt):
         (gs, us), (gn, un) = prev, nxt
@@ -663,22 +748,45 @@
             return
         spread(pos, v[0:3], (gtsum_ref, utsum_ref), (gtnext_ref, utnext_ref))
 
-    for k in range(1, NZ):
-        got(("tf", k), tfr.at[k])
-    for k in range(1, NT):
-        got(("eg", k), eg_ref.at[strip(lax.rem(t + k, NT))])
-    for i in range(3):
+    def tf_take():
+        for k in range(1, NZ):
+            got(("tf", k), tfr.at[k])
+
+    def fin_take(i):
         for k in range(1, NZ):
             got(("fin", i, k), finr.at[k, i])
-    pulls[5].wait()
-    pulls[6].wait()
-    for i, tiles in enumerate(((7, 8, 9, 10), (0, 3, 1, 4), (2, 5, 6))):
+
+    def write_out(i):
+        tiles = ((0, 1, 2, 3), (7, 8, 9, 10), (4, 5, 6))[i]
         for q, n in enumerate(tiles):
             k = lax.rem(q + NZ - z, NZ)
             tile_out(n, finr[k, i].astype(F32))
             taps_out(n, tfr[k, i])
-    for c in sent:
-        c.wait_send()
+
+    def sends_done():
+        for c in sent:
+            c.wait_send()
+
+    pulls[5].wait()
+    pulls[6].wait()
+    tf_take()
+    fin_take(0)
+    write_out(0)
+    fin_take(1)
+    write_out(1)
+    eg_last()
+    fin_take(2)
+    write_out(2)
+    sends_done()
+
+
+def flush(*refs):
+    sem = refs[12]
+    copies = [pltpu.make_async_copy(refs[n], refs[6 + n], sem.at[n]) for n in (1, 0, 2, 3, 4, 5)]
+    for c in copies:
+        c.start()
+    for c in copies:
+        c.wait()
 
 
 def per_device(
@@ -703,12 +811,12 @@
         ((3, HALF), F32),
         ((3, HALF), F32),
     )
-    n_sem = 190
+    n_sem = 240
     hbm = pl.BlockSpec(memory_space=pltpu.HBM)
     hid, *rest = pl.pallas_call(
         kernel,
         out_shape=[pltpu.VMEM(s, d) for s, d in shapes],
-        in_specs=[hbm] * 7 + [vmem] * 4,
+        in_specs=[hbm] * 11,
         out_specs=[vmem] * 6,
         scratch_shapes=[
             pltpu.VMEM((ROWS, 2048), BF16),
@@ -718,9 +826,14 @@
             pltpu.VMEM((64, HALF), BF16),
             pltpu.VMEM((64, HALF), F32),
             pltpu.VMEM((64, HALF), F32),
+            pltpu.VMEM((3, HALF), BF16),
+            pltpu.VMEM((3, HALF), BF16),
+            pltpu.VMEM((3, HALF), F32),
+            pltpu.VMEM((3, HALF), F32),
             pltpu.VMEM((64, LANE), F32),
             pltpu.VMEM((8, WIDE), F32),
             pltpu.VMEM((NY, 256, CA), BF16),
+            pltpu.VMEM((NY, 256, CC), BF16),
             pltpu.VMEM((NY, 256, CB), BF16),
             pltpu.VMEM((NY, ROWS, 256), BF16),
             pltpu.VMEM((NY, ROWS, 256), BF16),
@@ -736,14 +849,16 @@
             pltpu.VMEM((3, 256, LANE), BF16),
             pltpu.VMEM((NZ, 3, 64, LANE), BF16),
             pltpu.VMEM((ROWS, 2048), BF16),
-            pltpu.VMEM((NT, 32, 2048), BF16),
+            pltpu.VMEM((4, 32, 2048), BF16),
+            pltpu.VMEM((4, 32, 2048), BF16),
+            pltpu.VMEM((4, 32, 2048), BF16),
             pltpu.VMEM((32, 2048), BF16),
             pltpu.VMEM((NZ, 3, 8, LANE), F32),
             pltpu.VMEM((NZ, 3, 8, LANE), F32),
             pltpu.VMEM((3, 8, LANE), F32),
             pltpu.VMEM((NY, 3, 8, LANE), F32),
             pltpu.VMEM((NZ, 3, 8, LANE), F32),
-            pltpu.SemaphoreType.DMA((7,)),
+            pltpu.SemaphoreType.DMA((11,)),
             pltpu.SemaphoreType.DMA((n_sem,)),
             pltpu.SemaphoreType.DMA((n_sem,)),
         ],
@@ -763,6 +878,14 @@
         gate_taps_sum,
         up_taps_sum,
     )
+    hid, *rest = pl.pallas_call(
+        flush,
+        out_shape=[jax.ShapeDtypeStruct(s, d) for s, d in shapes],
+        in_specs=[vmem] * 6,
+        out_specs=[hbm] * 6,
+        scratch_shapes=[pltpu.SemaphoreType.DMA((6,))],
+        compiler_params=pltpu.CompilerParams(vmem_limit_bytes=8 * 1024 * 1024),
+    )(hid, *rest)
     return (hid.T, *rest)
 
 

time: 108 us -> 98 us (0.907)
  Pallas kernels: 102 us -> 96.6 us
  local copies, waits for them, and re-layouts: 4.26 us -> 0 us
    pallas_call x1, Pallas kernels: 102 us -> 95.3 us  [per_device(): pl.pallas_call(kernel, out_shape=[pltpu.VMEM(s, d) for s, d in shapes], i...]
    unnamed x6 -> x0, local copies, waits for them, and re-layouts: 4.26 us -> none
    pallas_call x0 -> x1, Pallas kernels: none -> 1.27 us  [per_device(): pl.pallas_call(flush, out_shape=[jax.ShapeDtypeStruct(s, d) for s, d in s...]
where the time goes in v3:
time: 98 us; the launch traced here: 97.2 us
  Pallas kernels  96.6 us (99%)
    pallas_call x1, Pallas kernels, per_device(): pl.pallas_call(kernel, out_shape=[pltpu.VMEM(s, d) for s, d in shapes], i...  95.3 us

profile of v3, /device:TPU:6, one launch (start us, length us, event | category | flops | bytes accessed | tf_op | source)
XLA Modules:
  0.0 97.2 jit_solution(17002645182315417242)
XLA Ops:
  0.6 95.3 %shard_map.154 = (bf16[704,256]{1,0:T(8,128)(2,1)S(1)}, bf16[256,2048]{1,0:T(8,128)(2,1)S(1)}, f32[64,704]{1,0:T(8,128)S(1)}, f32[64,704]{1,0:T(8,128)S(1)}, f32[3,704]{1,0:T(4,128)S(1)}, /*index=5*/f32[3,704]{1,0:T(4,128)S(1)}) custom-call(bf16[256,2048]{1,0:T(8,128)(2,1)} %late_hbm.1, bf16[256,2048]{1,0:T(8,128)(2,1)} %early_hbm.1, ...), custom_call_target="tpu_custom_call" | custom-call | tf_op jit(solution)/shard_map/pallas_call | solution.py:816
  96.0 1.3 %shard_map.155 = (bf16[704,256]{1,0:T(8,128)(2,1)}, bf16[256,2048]{1,0:T(8,128)(2,1)}, f32[64,704]{1,0:T(8,128)}, f32[64,704]{1,0:T(8,128)}, f32[3,704]{1,0:T(4,128)}, /*index=5*/f32[3,704]{1,0:T(4,128)}) custom-call(bf16[704,256]{1,0:T(8,128)(2,1)S(1)} %get-tuple-element.18.refs_0_, bf16[256,2048]{1,0:T(8,128)(2,1)S(1)} %get-tuple-element.19.refs_1_, ...), custom_call_target="tpu_custom_call" | custom-call | tf_op jit(solution)/shard_map/pallas_call | solution.py:881

commit v4 on v3

--- a/solution.py
+++ b/solution.py
@@ -69,12 +69,13 @@
     ut_hbm,
     gtsum_hbm,
     utsum_hbm,
-    hid_ref,
+    hid_out,
     eg_ref,
     gnext_ref,
     unext_ref,
     gtnext_ref,
     utnext_ref,
+    hid_ref,
     late_ref,
     early_ref,
     cot_ref,
@@ -172,30 +173,60 @@
         c.start()
         pulls.append(c)
 
-    slots = {}
-    sent = []
-
-    def slot(name):
-        return slots.setdefault(name, len(slots))
-
-    def copy_of(name, src, dst, dev):
-        k = slot(name)
+    arrivals, kinds = {}, {}
+
+    def arrival(name):
+        kind, rest = name[0], name[1:]
+        if kind == "a1":
+            rest = (rest[0], abs(rest[1]))
+        elif kind == "a2":
+            rest = (rest[0], rest[2], rest[3])
+        elif kind == "b1":
+            rest = (rest[1],)
+        elif kind in ("b2", "b2f"):
+            rest = (abs(rest[0]),)
+        elif kind in ("xx", "xf"):
+            rest = (rest[1],)
+        elif kind in ("dp", "fin"):
+            rest = (rest[0],)
+        elif kind == "rs":
+            rest = (rest[0], rest[1] % 3, rest[2])
+        elif kind != "xz":
+            rest = ()
+        return arrivals.setdefault((kind, *rest), len(arrivals))
+
+    def kind_of(name):
+        kind = name[0]
+        if kind in ("a1", "a2"):
+            kind += name[1]
+        elif kind in ("xz", "xx", "xf", "xc"):
+            kind = "x"
+        elif kind in ("dc", "dx", "eg", "ec"):
+            kind = "d"
+        elif kind in ("tz", "tf"):
+            kind = "t"
+        elif kind == "dp":
+            kind = "rs"
+        return kinds.setdefault(kind, len(kinds))
+
+    def copy_of(src, dst, s, r, dev):
         return pltpu.make_async_remote_copy(
             src_ref=src,
             dst_ref=dst,
-            send_sem=ssem.at[k],
-            recv_sem=rsem.at[k],
+            send_sem=ssem.at[s],
+            recv_sem=rsem.at[r],
             device_id=dev,
             device_id_type=MESH,
         )
 
     def send(name, src, dst, dev):
-        c = copy_of(name, src, dst, dev)
-        c.start()
-        sent.append(c)
-
-    def got(name, dst):
-        copy_of(name, dst, dst, ydev(1)).wait_recv()
+        copy_of(src, dst, kind_of(name), arrival(name), dev).start()
+
+    def got(name, ref):
+        copy_of(ref, ref, 0, arrival(name), ydev(1)).wait_recv()
+
+    def gone(kind, ref):
+        copy_of(ref, ref, kinds[kind], 0, ydev(1)).wait_send()
 
     def wrow(zz, first, n):
         return pl.ds(al(zz * 64 + first, 32), n)
@@ -286,56 +317,46 @@
         send(("xc", 0, j), blk, blk, pair)
 
     def x_mid(j):
+        got(("xx", 2, j), xt.at[0, pl.ds(0, 2)])
         for k, h in ((2, 0), (6, 128)):
             row = lax.rem(t + NT - k, NT)
             blk = xt.at[row, j]
-            got(("xx", k, j), blk)
             half = xt.at[row, j, pl.ds(h, 128)]
             send(("xf", k, j), half, half, tdev(k))
             send(("xc", k, j), blk, blk, pair)
 
     def x_far(j):
         row = lax.rem(t + 4, NT)
-        for k, h in ((2, 0), (6, 128)):
-            got(("xf", k, j), xt.at[row, j, pl.ds(h, 128)])
         blk = xt.at[row, j]
+        got(("xf", 2, j), blk)
         send(("xc", 4, j), blk, blk, pair)
 
     def x_last():
-        for j in range(1, NZ):
-            for k in (0, 2, 6, 4):
-                row = lax.rem(t + 1 - 2 * lax.rem(t, 2) + NT - k, NT)
-                got(("xc", k, j), xt.at[row, j])
+        got(("xc", 0, 1), xt.at[pl.ds(0, 4), pl.ds(0, 3)])
 
     def a1_near(p):
-        for k in (1, -1):
-            got(("a1", p, k), wide[p].at[y, wrow(zat(-k), 0, 64)])
+        got(("a1", p, 1), wide[p].at[0, pl.ds(0, 128)])
 
     def a1_far(p):
-        got(("a1", p, 2), wide[p].at[y, wrow(zat(2), 0, 32)])
-        got(("a1", p, -2), wide[p].at[y, wrow(zat(2), 32, 32)])
+        got(("a1", p, 2), wide[p].at[0, pl.ds(0, 64)])
 
     def a2_last(d):
         return (0, 1) if d == 1 else (2, 3)
 
     def a2_take(p, s, qs):
         for q in qs:
+            got(("a2", p, 1, s - 1, q), wide[p].at[0, pl.ds(0, 64 if s == 4 else 128)])
             for d in (1, -1):
-                if s == 4 and q not in a2_last(d):
-                    continue
                 blk = wide[p].at[yat(-d * s), wrow(zrow(q), 0, 64)]
-                got(("a2", p, d, s - 1, q), blk)
                 if s < 3 or (s == 3 and q in a2_last(d)):
                     send(("a2", p, d, s, q), blk, blk, ydev(d))
 
     def b1_take(s):
+        got(("b1", 1, s - 1, 0), wb.at[0, pl.ds(0, 64 if s == 4 else 128)])
         for d in (1, -1):
             mine = 0 if d == 1 else 1
             for h in (mine, 1 - mine):
-                if s == 4 and h != mine:
-                    continue
                 blk = wb.at[yat(-d * s), wrow(z, 32 * h, 32)]
-                got(("b1", d, s - 1, h), blk)
                 if s < 3 or (s == 3 and h == mine):
                     send(("b1", d, s, h), blk, blk, ydev(d))
         for e in ordinals(s):
@@ -347,18 +368,15 @@
         return (0,) if s == 0 else ((4,) if s == 4 else (s, -s))
 
     def b2_take(s):
+        got(("b2", s, 1), wb.at[0, pl.ds(0, 128 * len(ordinals(s)))])
         for e in ordinals(s):
             for k in (1, -1):
                 yb = yat(-e)
-                got(("b2", e, k), wb.at[yb, wrow(zat(-k), 0, 64)])
                 half = wb.at[yb, wrow(zat(-k), 0 if k == 1 else 32, 32)]
                 send(("b2f", e, k), half, half, ring(k))
 
     def b2f_take(s):
-        for e in ordinals(s):
-            yb = yat(-e)
-            got(("b2f", e, 1), wb.at[yb, wrow(zat(2), 0, 32)])
-            got(("b2f", e, -1), wb.at[yb, wrow(zat(2), 32, 32)])
+        got(("b2f", s, 1), wb.at[0, pl.ds(0, 64 * len(ordinals(s)))])
 
     def project(w, first, width, yb, start):
         rows = xe[yb]
@@ -485,8 +503,8 @@
             send(("dc", x), dxp.at[strip(2 * x + 1 - core)], dxc.at[x], pair)
 
     def dx_pair():
+        got(("dc", 0), dxc)
         for x in range(4):
-            got(("dc", x), dxc.at[x])
             v = dxp[strip(2 * x + core), :].astype(F32) + dxc[x].astype(F32)
             dxs[x] = v.astype(BF16)
         for k in (2, 6, 4):
@@ -494,8 +512,7 @@
             send(("dx", k), dxs.at[to], dxr.at[k // 2], tdev(-k))
 
     def taps_first():
-        for k in range(1, NZ):
-            got(("tz", k), tzr.at[k])
+        got(("tz", 1), tzr.at[pl.ds(1, 3)])
         tys[...] = tsum[z] + tzr[1] + tzr[2] + tzr[3]
         for k in range(1, NY):
             send(("ty", k), tys, tyr.at[k], ydev(-k))
@@ -514,8 +531,7 @@
 
     def rs(i, s):
         if s == 0:
-            for k in range(1, NZ):
-                got(("dp", i, k), dpg.at[i, k])
+            got(("dp", i, 1), dpg.at[i, pl.ds(1, 3)])
             for d in (1, -1):
                 buf = snd.at[side(d), i, 0]
                 buf[...] = term(i, yat(3 * d)).astype(BF16)
@@ -529,13 +545,14 @@
         if s < 3:
             for d in (1, -1):
                 v = term(i, yat(d * (3 - s)))
-                got(("rs", i, s - 1, d), rcv.at[side(d), i, s - 1])
+                if s == 1:
+                    got(("rs", i, 0, d), xt.at[0, 0, pl.ds(0, 192)])
+                else:
+                    got(("rs", i, s - 1, d), rcv.at[side(d), i, s - 1])
                 v = v + rcv[side(d), i, s - 1].astype(F32)
                 buf = snd.at[side(d), i, s]
                 if s == 1:
-                    far = rcv.at[side(d), i, 3, part(d)]
-                    got(("rs", i, 3, d), far)
-                    w = far[...].astype(F32)
+                    w = rcv[side(d), i, 3, part(d), :].astype(F32)
                     if d == 1:
                         buf[0:128, :] = (v[0:128] + w).astype(BF16)
                         buf[128:256, :] = v[128:256].astype(BF16)
@@ -555,10 +572,16 @@
             send(("fin", i, k), fin.at[i, wrow(zat(-k), 0, 64)], finr.at[k, i], zdev(-k))
         finr[0, i] = fin[i, own, :]
 
+    def eg_own():
+        return pltpu.make_async_copy(egs, eg_ref.at[strip(t)], lsem.at[11])
+
+    def hid_flush():
+        return pltpu.make_async_copy(hid_ref, hid_out, lsem.at[12])
+
     def dx_reduce():
         v = dxs[lax.div(t, 2)].astype(F32)
+        got(("dx", 2), dxr.at[pl.ds(1, 3)])
         for k in (2, 6, 4):
-            got(("dx", k), dxr.at[k // 2])
             v = v + dxr[k // 2].astype(F32)
         for yp in range(NY // 2):
             for zp in range(2):
@@ -571,23 +594,21 @@
         for k in (2, 6, 4):
             send(("eg", k), egs, eg_ref.at[strip(t)], tdev(k))
         send(("ec", 0), egs, eg_ref.at[strip(t)], pair)
-        eg_ref[strip(t), :] = egs[...]
+        eg_own().start()
 
     def eg_cross():
+        got(("eg", 2), dxr.at[pl.ds(1, 3)])
         for k in (2, 6, 4):
             here = eg_ref.at[strip(lax.rem(t + NT - k, NT))]
-            got(("eg", k), here)
             send(("ec", k), here, here, pair)
 
     def eg_last():
-        for k in (0, 2, 6, 4):
-            row = lax.rem(t + 1 - 2 * lax.rem(t, 2) + NT - k, NT)
-            got(("ec", k), eg_ref.at[strip(row)])
+        got(("ec", 0), dxc)
 
     def taps_finish():
         v = tys[...]
+        got(("ty", 1), tyr.at[pl.ds(1, 7)])
         for k in range(1, NY):
-            got(("ty", k), tyr.at[k])
             v = v + tyr[k]
         tfr[0] = v
         for k in range(1, NZ):
@@ -651,74 +672,74 @@
     a2_own("c", 3)
     x_take(2)
     project_a(2)
+    b2_take(3)
+    x_take(3)
     a2_take("a", 4, range(NZ))
     a2_take("c", 1, (0,))
-    b2_take(3)
+    x_mid(1)
     project_a(3)
     a2_take("c", 1, (1,))
-    x_mid(1)
+    b2_take(4)
+    project_a(4)
+    a2_take("c", 1, (2,))
+    x_mid(2)
     pulls[4].wait()
     turn_cot()
     join_taps()
-    a2_take("c", 1, (2,))
-    project_a(4)
     lax.fori_loop(0, 2, early_a, 0)
     dp_send(0)
     a2_take("c", 1, (3,))
-    b2_take(4)
-    x_take(3)
-    a2_take("c", 2, (0,))
-    x_mid(2)
-    x_far(1)
-    a2_take("c", 2, (1,))
     b2f_take(0)
     project_b(0)
+    x_far(1)
     b2f_take(1)
     project_b(1)
-    a2_take("c", 2, (2, 3))
+    a2_take("c", 2, (0, 1))
+    x_mid(3)
     b2f_take(2)
     project_b(2)
-    a2_take("c", 3, (0,))
-    x_mid(3)
+    a2_take("c", 2, (2,))
     x_far(2)
-    project_c(0)
-    a2_take("c", 3, (1,))
+    a2_take("c", 2, (3,))
     b2f_take(3)
     project_b(3)
-    a2_take("c", 3, (2, 3))
     b2f_take(4)
     project_b(4)
+    a2_take("c", 3, (0,))
     lax.fori_loop(0, 2, early_b, 0)
     dp_send(1)
+    a2_take("c", 3, (1,))
+    x_far(3)
+    project_c(0)
+    a2_take("c", 3, (2, 3))
     project_c(1)
     project_c(2)
     project_c(3)
-    x_far(3)
+    x_last()
+    rs(0, 0)
     a2_take("c", 4, range(NZ))
     project_c(4)
     early_c()
     dp_send(2)
-    x_last()
-    rs(0, 0)
     lax.fori_loop(0, NY, dx, 0)
     dx_send()
+    rs(1, 0)
     rs(0, 1)
-    rs(1, 0)
     dx_pair()
     taps_first()
-    late_project(wa, 0, 0, 256)
+    rs(2, 0)
     rs(0, 2)
     rs(1, 1)
-    rs(2, 0)
+    late_project(wa, 0, 0, 256)
     late_project(wa, 0, 256, 256)
+    rs(2, 1)
     rs(0, 3)
     rs(1, 2)
-    rs(2, 1)
+    late_project(wc, CA, 0, 256)
     dx_reduce()
-    late_project(wc, CA, 0, 256)
+    rs(2, 2)
+    rs(1, 3)
     late_project(wc, CA, 256, 128)
-    rs(1, 3)
-    rs(2, 2)
     late_project(wb, AC, 0, 256)
     late_project(wb, AC, 256, 256)
     taps_finish()
@@ -727,6 +748,7 @@
     rs(2, 3)
     lax.fori_loop(0, 2, late_b, 0)
     late_c()
+    hid_flush().start()
 
     def spread(pos, v, prev, nxt):
         (gs, us), (gn, un) = prev, nxt
@@ -749,12 +771,10 @@
         spread(pos, v[0:3], (gtsum_ref, utsum_ref), (gtnext_ref, utnext_ref))
 
     def tf_take():
-        for k in range(1, NZ):
-            got(("tf", k), tfr.at[k])
+        got(("tf", 1), tfr.at[pl.ds(1, 3)])
 
     def fin_take(i):
-        for k in range(1, NZ):
-            got(("fin", i, k), finr.at[k, i])
+        got(("fin", i, 1), finr.at[pl.ds(1, 3), i])
 
     def write_out(i):
         tiles = ((0, 1, 2, 3), (7, 8, 9, 10), (4, 5, 6))[i]
@@ -764,8 +784,21 @@
             taps_out(n, tfr[k, i])
 
     def sends_done():
-        for c in sent:
-            c.wait_send()
+        eg_own().wait()
+        hid_flush().wait()
+        gone("a1a", wa.at[0, pl.ds(0, 192)])
+        gone("a1c", wc.at[0, pl.ds(0, 192)])
+        gone("a2a", wa.at[pl.ds(0, 7)])
+        gone("a2c", wc.at[pl.ds(0, 7)])
+        gone("b1", wb.at[pl.ds(0, 7), pl.ds(0, 64)])
+        gone("b2", wb.at[pl.ds(0, 4)])
+        gone("b2f", wb.at[pl.ds(0, 2)])
+        gone("x", xt.at[pl.ds(0, 6)])
+        gone("rs", xt.at[pl.ds(0, 5), pl.ds(0, 3)])
+        gone("fin", finr.at[pl.ds(0, 3)])
+        gone("t", tyr.at[pl.ds(0, 6)])
+        gone("ty", tyr.at[pl.ds(0, 7)])
+        gone("d", xt.at[pl.ds(0, 7), pl.ds(0, 2)])
 
     pulls[5].wait()
     pulls[6].wait()
@@ -811,14 +844,15 @@
         ((3, HALF), F32),
         ((3, HALF), F32),
     )
-    n_sem = 240
+    n_sem = 91
     hbm = pl.BlockSpec(memory_space=pltpu.HBM)
     hid, *rest = pl.pallas_call(
         kernel,
         out_shape=[pltpu.VMEM(s, d) for s, d in shapes],
         in_specs=[hbm] * 11,
-        out_specs=[vmem] * 6,
+        out_specs=[pl.BlockSpec(memory_space=pl.ANY)] * 2 + [vmem] * 4,
         scratch_shapes=[
+            pltpu.VMEM((HALF, ROWS), BF16),
             pltpu.VMEM((ROWS, 2048), BF16),
             pltpu.VMEM((ROWS, 2048), BF16),
             pltpu.VMEM((HALF, ROWS), BF16),
@@ -858,8 +892,8 @@
             pltpu.VMEM((3, 8, LANE), F32),
             pltpu.VMEM((NY, 3, 8, LANE), F32),
             pltpu.VMEM((NZ, 3, 8, LANE), F32),
-            pltpu.SemaphoreType.DMA((11,)),
-            pltpu.SemaphoreType.DMA((n_sem,)),
+            pltpu.SemaphoreType.DMA((13,)),
+            pltpu.SemaphoreType.DMA((13,)),
             pltpu.SemaphoreType.DMA((n_sem,)),
         ],
         compiler_params=pltpu.CompilerParams(

time: 98 us -> 93.6 us (0.955)
  Pallas kernels: 96.6 us -> 91.9 us
    pallas_call x1, Pallas kernels: 95.3 us -> 90.6 us  [per_device(): pl.pallas_call(kernel, out_shape=[pltpu.VMEM(s, d) for s, d in shapes], i...]
where the time goes in v4:
time: 93.6 us; the launch traced here: 92.5 us
  Pallas kernels  91.9 us (98%)
    pallas_call x1, Pallas kernels, per_device(): pl.pallas_call(kernel, out_shape=[pltpu.VMEM(s, d) for s, d in shapes], i...  90.6 us

profile of v4, /device:TPU:6, one launch (start us, length us, event | category | flops | bytes accessed | tf_op | source)
XLA Modules:
  0.0 92.5 jit_solution(2716976549984752661)
XLA Ops:
  0.6 90.6 %shard_map.154 = (bf16[704,256]{1,0:T(8,128)(2,1)S(1)}, bf16[256,2048]{1,0:T(8,128)(2,1)S(1)}, f32[64,704]{1,0:T(8,128)S(1)}, f32[64,704]{1,0:T(8,128)S(1)}, f32[3,704]{1,0:T(4,128)S(1)}, /*index=5*/f32[3,704]{1,0:T(4,128)S(1)}) custom-call(bf16[256,2048]{1,0:T(8,128)(2,1)} %late_hbm.1, bf16[256,2048]{1,0:T(8,128)(2,1)} %early_hbm.1, ...), custom_call_target="tpu_custom_call" | custom-call | tf_op jit(solution)/shard_map/pallas_call | solution.py:849
  91.2 1.3 %shard_map.155 = (bf16[704,256]{1,0:T(8,128)(2,1)}, bf16[256,2048]{1,0:T(8,128)(2,1)}, f32[64,704]{1,0:T(8,128)}, f32[64,704]{1,0:T(8,128)}, f32[3,704]{1,0:T(4,128)}, /*index=5*/f32[3,704]{1,0:T(4,128)}) custom-call(bf16[704,256]{1,0:T(8,128)(2,1)S(1)} %get-tuple-element.18.refs_0_, bf16[256,2048]{1,0:T(8,128)(2,1)S(1)} %get-tuple-element.19.refs_1_, ...), custom_call_target="tpu_custom_call" | custom-call | tf_op jit(solution)/shard_map/pallas_call | solution.py:915

commit v5 on v4

--- a/solution.py
+++ b/solution.py
@@ -672,46 +672,47 @@
     a2_own("c", 3)
     x_take(2)
     project_a(2)
+    a2_take("c", 1, (0,))
+    a2_take("c", 1, (1,))
+    x_take(3)
+    a2_take("c", 1, (2,))
+    project_a(3)
     b2_take(3)
-    x_take(3)
+    a2_take("c", 1, (3,))
     a2_take("a", 4, range(NZ))
-    a2_take("c", 1, (0,))
     x_mid(1)
-    project_a(3)
-    a2_take("c", 1, (1,))
     b2_take(4)
+    a2_take("c", 2, (0,))
     project_a(4)
-    a2_take("c", 1, (2,))
     x_mid(2)
+    a2_take("c", 2, (1,))
     pulls[4].wait()
     turn_cot()
     join_taps()
     lax.fori_loop(0, 2, early_a, 0)
     dp_send(0)
-    a2_take("c", 1, (3,))
+    a2_take("c", 2, (2,))
     b2f_take(0)
     project_b(0)
     x_far(1)
+    a2_take("c", 2, (3,))
     b2f_take(1)
     project_b(1)
-    a2_take("c", 2, (0, 1))
     x_mid(3)
     b2f_take(2)
     project_b(2)
-    a2_take("c", 2, (2,))
+    a2_take("c", 3, (0,))
     x_far(2)
-    a2_take("c", 2, (3,))
     b2f_take(3)
     project_b(3)
+    a2_take("c", 3, (1,))
     b2f_take(4)
     project_b(4)
-    a2_take("c", 3, (0,))
+    a2_take("c", 3, (2, 3))
     lax.fori_loop(0, 2, early_b, 0)
     dp_send(1)
-    a2_take("c", 3, (1,))
     x_far(3)
     project_c(0)
-    a2_take("c", 3, (2, 3))
     project_c(1)
     project_c(2)
     project_c(3)
@@ -732,20 +733,20 @@
     rs(1, 1)
     late_project(wa, 0, 0, 256)
     late_project(wa, 0, 256, 256)
+    late_project(wc, CA, 0, 256)
+    late_project(wc, CA, 256, 128)
     rs(2, 1)
+    dx_reduce()
     rs(0, 3)
     rs(1, 2)
-    late_project(wc, CA, 0, 256)
-    dx_reduce()
+    late_project(wb, AC, 0, 256)
     rs(2, 2)
     rs(1, 3)
-    late_project(wc, CA, 256, 128)
-    late_project(wb, AC, 0, 256)
+    taps_finish()
     late_project(wb, AC, 256, 256)
-    taps_finish()
     eg_cross()
+    rs(2, 3)
     lax.fori_loop(0, 2, late_a, 0)
-    rs(2, 3)
     lax.fori_loop(0, 2, late_b, 0)
     late_c()
     hid_flush().start()

time: 93.6 us -> 89.3 us (0.954); the launches traced: 92.5 us -> 89.2 us
  Pallas kernels: 91.9 us -> 88.5 us
    pallas_call x1, Pallas kernels: 90.6 us -> 87.2 us  [per_device(): pl.pallas_call(kernel, out_shape=[pltpu.VMEM(s, d) for s, d in shapes], i...]
where the time goes in v5:
time: 89.3 us; the launch traced here: 89.2 us
  Pallas kernels  88.5 us (99%)
    pallas_call x1, Pallas kernels, per_device(): pl.pallas_call(kernel, out_shape=[pltpu.VMEM(s, d) for s, d in shapes], i...  87.2 us

profile of v5, /device:TPU:6, one launch (start us, length us, event | category | flops | bytes accessed | tf_op | source)
XLA Modules:
  0.0 89.2 jit_solution(14506364122136956614)
XLA Ops:
  0.6 87.2 %shard_map.154 = (bf16[704,256]{1,0:T(8,128)(2,1)S(1)}, bf16[256,2048]{1,0:T(8,128)(2,1)S(1)}, f32[64,704]{1,0:T(8,128)S(1)}, f32[64,704]{1,0:T(8,128)S(1)}, f32[3,704]{1,0:T(4,128)S(1)}, /*index=5*/f32[3,704]{1,0:T(4,128)S(1)}) custom-call(bf16[256,2048]{1,0:T(8,128)(2,1)} %late_hbm.1, bf16[256,2048]{1,0:T(8,128)(2,1)} %early_hbm.1, ...), custom_call_target="tpu_custom_call" | custom-call | tf_op jit(solution)/shard_map/pallas_call | solution.py:850
  87.9 1.3 %shard_map.155 = (bf16[704,256]{1,0:T(8,128)(2,1)}, bf16[256,2048]{1,0:T(8,128)(2,1)}, f32[64,704]{1,0:T(8,128)}, f32[64,704]{1,0:T(8,128)}, f32[3,704]{1,0:T(4,128)}, /*index=5*/f32[3,704]{1,0:T(4,128)}) custom-call(bf16[704,256]{1,0:T(8,128)(2,1)S(1)} %get-tuple-element.18.refs_0_, bf16[256,2048]{1,0:T(8,128)(2,1)S(1)} %get-tuple-element.19.refs_1_, ...), custom_call_target="tpu_custom_call" | custom-call | tf_op jit(solution)/shard_map/pallas_call | solution.py:916

commit v6 on v5

--- a/solution.py
+++ b/solution.py
@@ -532,15 +532,15 @@
     def rs(i, s):
         if s == 0:
             got(("dp", i, 1), dpg.at[i, pl.ds(1, 3)])
-            for d in (1, -1):
-                buf = snd.at[side(d), i, 0]
-                buf[...] = term(i, yat(3 * d)).astype(BF16)
-                send(("rs", i, 0, d), buf, rcv.at[side(d), i, 0], ydev(d))
             v = term(i, yat(4))
             for d in (1, -1):
                 buf = snd.at[side(d), i, 3, part(d)]
                 buf[...] = (v[0:128] if d == 1 else v[128:256]).astype(BF16)
                 send(("rs", i, 3, d), buf, rcv.at[side(d), i, 3, part(d)], ydev(2 * d))
+            for d in (1, -1):
+                buf = snd.at[side(d), i, 0]
+                buf[...] = term(i, yat(3 * d)).astype(BF16)
+                send(("rs", i, 0, d), buf, rcv.at[side(d), i, 0], ydev(d))
             return
         if s < 3:
             for d in (1, -1):
@@ -722,10 +722,11 @@
     project_c(4)
     early_c()
     dp_send(2)
-    lax.fori_loop(0, NY, dx, 0)
+    lax.fori_loop(0, 4, dx, 0)
+    rs(0, 1)
+    lax.fori_loop(4, NY, dx, 0)
     dx_send()
     rs(1, 0)
-    rs(0, 1)
     dx_pair()
     taps_first()
     rs(2, 0)

time: 89.3 us -> 90.1 us (level)
  no operation moved by 1% of the time
where the time goes in v6:
time: 90.1 us; the launch traced here: 89.3 us
  Pallas kernels  88.6 us (98%)
    pallas_call x1, Pallas kernels, per_device(): pl.pallas_call(kernel, out_shape=[pltpu.VMEM(s, d) for s, d in shapes], i...  87.4 us

profile of v6, /device:TPU:6, one launch (start us, length us, event | category | flops | bytes accessed | tf_op | source)
XLA Modules:
  0.0 89.3 jit_solution(15893861802734574838)
XLA Ops:
  0.6 87.4 %shard_map.154 = (bf16[704,256]{1,0:T(8,128)(2,1)S(1)}, bf16[256,2048]{1,0:T(8,128)(2,1)S(1)}, f32[64,704]{1,0:T(8,128)S(1)}, f32[64,704]{1,0:T(8,128)S(1)}, f32[3,704]{1,0:T(4,128)S(1)}, /*index=5*/f32[3,704]{1,0:T(4,128)S(1)}) custom-call(bf16[256,2048]{1,0:T(8,128)(2,1)} %late_hbm.1, bf16[256,2048]{1,0:T(8,128)(2,1)} %early_hbm.1, ...), custom_call_target="tpu_custom_call" | custom-call | tf_op jit(solution)/shard_map/pallas_call | solution.py:851
  88.0 1.3 %shard_map.155 = (bf16[704,256]{1,0:T(8,128)(2,1)}, bf16[256,2048]{1,0:T(8,128)(2,1)}, f32[64,704]{1,0:T(8,128)}, f32[64,704]{1,0:T(8,128)}, f32[3,704]{1,0:T(4,128)}, /*index=5*/f32[3,704]{1,0:T(4,128)}) custom-call(bf16[704,256]{1,0:T(8,128)(2,1)S(1)} %get-tuple-element.18.refs_0_, bf16[256,2048]{1,0:T(8,128)(2,1)S(1)} %get-tuple-element.19.refs_1_, ...), custom_call_target="tpu_custom_call" | custom-call | tf_op jit(solution)/shard_map/pallas_call | solution.py:917
